TPU v7x, 256 devices: a whole 4x4x8 slice. The times are simulated.
256 devices in a mesh: rep: 64 (over z, y, x_hi), fs: 2 (over core), tp: 2 (over x_lo).
Axes of the slice: x: 4 (x_hi: 2, x_lo: 2; x = x_hi * 2 + x_lo), y: 4, z: 8, core: 2. Of those that a mesh axis runs over, the one named last changes fastest.
Arguments:
- inputs: bfloat16 [16384, 2048], P(('rep', 'fs'), 'tp'), may hold values from -24 to 24
- cotangent: bfloat16 [16384, 2048], P(('rep', 'fs'), 'tp'), may hold values from -24 to 24
- w_up: bfloat16 [2048, 4096], P('fs', 'tp'), may hold values from -0.125 to 0.125
- w_down: bfloat16 [4096, 2048], P('tp', 'fs'), may hold values from -0.09375 to 0.09375
Outputs:
- grad_inputs: bfloat16 [16384, 2048], P(('rep', 'fs'), 'tp')
- grad_up: float32 [2048, 4096], P('fs', 'tp')
- grad_down: float32 [4096, 2048], P('tp', 'fs')
All inputs are finite; a program needn't handle non-finite values.
Results may differ from a plain program's by a relative error of at most 0.011.
Values may be sent and summed in bfloat16 or wider, within the bound.
A program may use at most 128 MiB of HBM per device.

v0:
```python
import jax
import jax.numpy as jnp
from jax import lax
from jax.sharding import PartitionSpec as P


def from_everyone(shard, axis):
    devices = lax.axis_size(axis)
    return lax.all_to_all(
        jnp.broadcast_to(shard[None], (devices, *shard.shape)), axis, 0, 0, tiled=True
    )


def joined_along(pieces, dim):
    pieces = jnp.moveaxis(pieces, 0, dim)
    lengths = pieces.shape
    return pieces.reshape(*lengths[:dim], lengths[dim] * lengths[dim + 1], *lengths[dim + 2 :])


def gathered_copies(shard, axis, dim):
    pieces = from_everyone(shard, axis)
    return joined_along(pieces, dim)


def side_by_side(arrays, axis, dim, along):
    both = jnp.concatenate(arrays, axis=along)
    result, at, outs = (gathered_copies(both, axis, dim), 0, [])
    for a in arrays:
        outs.append(lax.slice_in_dim(result, at, at + a.shape[along], axis=along))
        at += a.shape[along]
    return tuple(outs)


def cut_along(shard, dim, devices):
    before, after = (shard.shape[:dim], shard.shape[dim + 1 :])
    return jnp.moveaxis(shard.reshape(*before, devices, -1, *after), dim, 0)


def sent_and_summed(shard, axis, dim):
    pieces = cut_along(shard, dim, lax.axis_size(axis))
    arrived = lax.all_to_all(pieces, axis, split_axis=0, concat_axis=0, tiled=True)
    return arrived.astype(jnp.float32).sum(axis=0)


def in_one_piece(arrays, axis, dim, along):
    ends, at = ([], 0)
    for a in arrays[:-1]:
        at += a.shape[along]
        ends.append(at)
    both = jnp.concatenate(arrays, axis=along)
    return tuple(jnp.split(lax.all_gather(both, axis, axis=dim, tiled=True), ends, axis=along))


def gather_packed(arrays, axis, dims):
    flat = jnp.concatenate([a.reshape(-1) for a in arrays])
    lines, at, outs = (lax.all_gather(flat, axis), 0, [])
    for a, dim in zip(arrays, dims):
        pieces = lines[:, at : at + a.size].reshape(-1, *a.shape)
        outs.append(joined_along(pieces, dim))
        at += a.size
    return tuple(outs)


def contract_rows(left, right):
    return lax.dot_general(
        left, right, (((0,), (0,)), ((), ())), preferred_element_type=jnp.float32
    )


def contract_cols(left, right):
    return lax.dot_general(
        left, right, (((1,), (1,)), ((), ())), preferred_element_type=jnp.float32
    )


def shards(inputs, cotangent, w_up, w_down):
    rows_in, rows_cot = side_by_side((inputs, cotangent), "tp", 1, 0)
    cols_in, cols_cot = (
        lax.all_to_all(rows_in, "fs", split_axis=1, concat_axis=0, tiled=True),
        lax.all_to_all(rows_cot, "fs", split_axis=1, concat_axis=0, tiled=True),
    )
    full_up = lax.all_gather(w_up, "fs", axis=0, tiled=True)
    act_grad = sent_and_summed(contract_cols(cols_cot, w_down).astype(jnp.bfloat16), "fs", 0)
    preact = jnp.dot(rows_in, full_up, preferred_element_type=jnp.float32)
    relu_pre = jnp.maximum(preact, 0.0)
    squared = (relu_pre * relu_pre).astype(jnp.bfloat16)
    pre_grad = (2.0 * relu_pre * act_grad).astype(jnp.bfloat16)
    partial_value = contract_cols(pre_grad, full_up)
    grad_inputs = sent_and_summed(partial_value.astype(jnp.bfloat16), "tp", 1).astype(jnp.bfloat16)
    grad_piece, square_piece = in_one_piece((pre_grad, squared), "fs", 0, 1)
    local_up = contract_rows(cols_in, grad_piece)
    local_down = contract_rows(square_piece, cols_cot)
    slice_up = sent_and_summed(local_up.astype(jnp.bfloat16), "rep", 0)
    slice_down = sent_and_summed(local_down.astype(jnp.bfloat16), "rep", 0)
    grad_up, grad_down = gather_packed((slice_up, slice_down), "rep", (0, 0))
    return (grad_inputs, grad_up, grad_down)


def solution(mesh):
    return jax.shard_map(
        shards,
        mesh=mesh,
        in_specs=(P(("rep", "fs"), "tp"), P(("rep", "fs"), "tp"), P("fs", "tp"), P("tp", "fs")),
        out_specs=(P(("rep", "fs"), "tp"), P("fs", "tp"), P("tp", "fs")),
        check_vma=False,
    )
```

profile of v0, /device:TPU:8, one launch (start us, length us, event | category | flops | bytes accessed | tf_op | source)
XLA Modules:
  0.0 542.4 jit_solution(15013829221324281810)
XLA Ops:
  7.2 0.0 copy-start.2
  7.2 0.0 copy-start.3
  7.2 0.0 all-gather.5.cloned.1.call-start
  7.2 0.7 all-gather.5.cloned.1.call-update
  7.9 0.0 all-gather.7.cloned.1.call-start
  8.0 0.1 copy-done.2
  8.1 0.1 copy-done.3
  8.2 0.2 copy.11
  8.4 0.1 broadcast_in_dim.2
  8.5 16.3 %all_to_all.57 = bf16[2,256,1024]{1,2,0:T(8,128)(2,1)S(1)} all-to-all(bf16[2,256,1024]{1,2,0:T(8,128)(2,1)S(1)} %broadcast_in_dim.2), channel_id=1, replica_groups=mesh['rep'=64,'fs'=2,'tp'=2] {'tp'}, dimensions={0} | all-to-all | bytes 2097152 | tf_op jit(solution)/shard_map/all_to_all | solution.py:9
  24.8 1.0 fusion.3
  25.8 4.2 all_to_all.58
  30.0 0.2 copy.12
  30.2 3.9 convolution_convert_fusion.2
  34.1 4.6 all_to_all.59
  38.6 0.2 convert_reduce_fusion.2
  38.8 0.0 all-gather.5.cloned.1.call-done
  38.9 4.9 multiply_convert_fusion
  43.8 1.0 pad_maximum_fusion
  44.8 0.0 all-gather.7.cloned.1.call-update
  44.8 3.5 all-to-all-start.4
  48.3 16.1 %all-gather.7.cloned.1.call-done = bf16[256,4096]{1,0:T(8,128)(2,1)} async-done(((bf16[128,4096]{1,0:T(8,128)(2,1)}), bf16[256,4096]{1,0:T(8,128)(2,1)}) %all-gather.7.cloned.1.call-update) | async-done | bytes 2097168 | tf_op jit(solution)/shard_map/all_gather | solution.py:51
  64.5 4.5 convolution_convert_fusion
  69.0 0.0 all-to-all-done.4
  69.0 0.0 copy-start.1
  69.0 0.0 copy-start
  69.0 0.8 copy-done.1
  69.8 13.3 %all-to-all-start.6 = ((bf16[64,32,1024]{2,1,0:T(8,128)(2,1)}), bf16[64,32,1024]{2,1,0:T(8,128)(2,1)}, u32[]{:S(2)}, u32[]{:S(2)}) async-start(bf16[64,32,1024]{2,1,0:T(8,128)(2,1)} %bitcast.28), calls=%async_computation.6 | async-start | bytes 8388608 | tf_op jit(solution)/shard_map/all_to_all | solution.py:41
  83.1 1.2 copy.14
  84.3 0.0 copy-done
  84.3 3.3 convolution_convert_fusion.1
  87.7 91.3 %all-to-all-done.6 = bf16[64,32,1024]{2,1,0:T(8,128)(2,1)} async-done(((bf16[64,32,1024]{2,1,0:T(8,128)(2,1)}), bf16[64,32,1024]{2,1,0:T(8,128)(2,1)}, u32[]{:S(2)}, u32[]{:S(2)}) %all-to-all-start.6) | async-done | bytes 4194336 | tf_op jit(solution)/shard_map/all_to_all | solution.py:41
  179.0 8.3 %all-to-all-start.5 = ((bf16[64,16,2048]{2,1,0:T(8,128)(2,1)}), bf16[64,16,2048]{2,1,0:T(8,128)(2,1)}, u32[]{:S(2)}, u32[]{:S(2)}) async-start(bf16[64,16,2048]{2,1,0:T(8,128)(2,1)} %bitcast.29), calls=%async_computation.5 | async-start | bytes 8388608 | tf_op jit(solution)/shard_map/all_to_all | solution.py:41
  187.3 0.2 all-gather.9.cloned.1.call-start
  187.5 3.0 convert_reduce_fusion
  190.6 91.3 %all-to-all-done.5 = bf16[64,16,2048]{2,1,0:T(8,128)(2,1)} async-done(((bf16[64,16,2048]{2,1,0:T(8,128)(2,1)}), bf16[64,16,2048]{2,1,0:T(8,128)(2,1)}, u32[]{:S(2)}, u32[]{:S(2)}) %all-to-all-start.5) | async-done | bytes 4194336 | tf_op jit(solution)/shard_map/all_to_all | solution.py:41
  282.0 2.9 convert_reduce_fusion.1
  284.8 0.7 pad_maximum_fusion.2
  285.6 0.0 all-gather.9.cloned.1.call-update
  285.6 6.3 %convolution_convert_fusion.3 = bf16[128,2048]{1,0:T(8,128)(2,1)S(1)} fusion(bf16[128,2048]{1,0:T(8,128)(2,1)S(1)} %get-tuple-element.6, bf16[2048,2048]{1,0:T(8,128)(2,1)} %all-gather.5.cloned.1.call-done), kind=kOutput, calls=%fused_computation.6 | convolution fusion | flops 1074003968 | bytes 9437184 | tf_op jit(solution)/shard_map/dot_general | solution.py:71
  291.9 10.9 %all_to_all.60 = bf16[2,128,1024]{2,1,0:T(8,128)(2,1)S(1)} all-to-all(bf16[2,128,1024]{2,1,0:T(8,128)(2,1)S(1)} %bitcast.37), channel_id=1, replica_groups=mesh['rep'=64,'fs'=2,'tp'=2] {'tp'}, dimensions={0} | all-to-all | bytes 1048576 | tf_op jit(solution)/shard_map/all_to_all | solution.py:41
  302.8 0.8 reduce_sum.40
  303.6 187.4 %all-gather.9.cloned.1.call-done = f32[4194304]{0:T(1024)} async-done(((f32[65536]{0:T(1024)}), f32[4194304]{0:T(1024)}) %all-gather.9.cloned.1.call-update) | async-done | bytes 16777232 | tf_op jit(solution)/shard_map/all_gather | solution.py:56
  491.0 14.5 %reshape.42 = f32[64,65536]{1,0:T(8,128)} reshape(f32[4194304]{0:T(1024)} %all-gather.9.cloned.1.call-done) | data formatting | bytes 33554432 | tf_op jit(solution)/shard_map/all_gather | solution.py:56
  505.5 11.7 %fusion.2 = (f32[64,32768]{1,0:T(8,128)}, f32[64,32768]{1,0:T(8,128)}) fusion(f32[64,65536]{1,0:T(8,128)} %reshape.42), kind=kLoop, calls=%fused_computation.16 | loop fusion | bytes 33554432 | tf_op jit(solution)/shard_map/slice | solution.py:58
  517.2 9.4 %reshape_reshape.7 = f32[2048,1024]{1,0:T(8,128)} reshape(f32[64,32768]{1,0:T(8,128)} %get-tuple-element.3) | data formatting | bytes 16777216 | tf_op jit(solution)/shard_map/reshape;reshape | solution.py:17
  526.5 9.4 %reshape_reshape.6 = f32[1024,2048]{1,0:T(8,128)} reshape(f32[64,32768]{1,0:T(8,128)} %get-tuple-element.4) | data formatting | bytes 16777216 | tf_op jit(solution)/shard_map/reshape;reshape | solution.py:17
  (4 shorter events, 0.1 us)
Async XLA Ops:
  7.2 1.0 copy-start.2
  7.2 1.0 copy-start.3
  7.2 31.7 %all-gather.5.cloned.1.call-start = ((), (), s32[]{:S(2)}) async-start(), calls=%async_computation.7 | async-start | bytes 12582912 | tf_op jit(solution)/shard_map/all_gather | solution.py:82
  7.9 56.5 %all-gather.7.cloned.1.call-start = ((), (), s32[]{:S(2)}) async-start(), calls=%async_computation.8 | async-start | bytes 3145728 | tf_op jit(solution)/shard_map/all_gather | solution.py:51
  44.8 24.2 %all-to-all-start.4 = ((bf16[128,2,1024]{0,2,1:T(8,128)(2,1)}), bf16[128,2,1024]{0,2,1:T(8,128)(2,1)S(1)}, u32[]{:S(2)}, u32[]{:S(2)}) async-start(bf16[128,2,1024]{0,2,1:T(8,128)(2,1)} %get-tuple-element.7), calls=%async_computation.4 | async-start | bytes 1048576 | tf_op jit(solution)/shard_map/all_to_all | solution.py:79
  69.0 0.8 copy-start.1
  69.0 15.3 %copy-start = (bf16[256,4096]{1,0:T(8,128)(2,1)S(1)}, bf16[256,4096]{1,0:T(8,128)(2,1)}, u32[]{:S(2)}) copy-start(bf16[256,4096]{1,0:T(8,128)(2,1)} %all-gather.7.cloned.1.call-done) | copy-start | bytes 6291460
  69.8 109.2 %all-to-all-start.6 = ((bf16[64,32,1024]{2,1,0:T(8,128)(2,1)}), bf16[64,32,1024]{2,1,0:T(8,128)(2,1)}, u32[]{:S(2)}, u32[]{:S(2)}) async-start(bf16[64,32,1024]{2,1,0:T(8,128)(2,1)} %bitcast.28), calls=%async_computation.6 | async-start | bytes 8388608 | tf_op jit(solution)/shard_map/all_to_all | solution.py:41
  179.0 103.0 %all-to-all-start.5 = ((bf16[64,16,2048]{2,1,0:T(8,128)(2,1)}), bf16[64,16,2048]{2,1,0:T(8,128)(2,1)}, u32[]{:S(2)}, u32[]{:S(2)}) async-start(bf16[64,16,2048]{2,1,0:T(8,128)(2,1)} %bitcast.29), calls=%async_computation.5 | async-start | bytes 8388608 | tf_op jit(solution)/shard_map/all_to_all | solution.py:41
  187.3 303.7 %all-gather.9.cloned.1.call-start = ((), (), s32[]{:S(2)}) async-start(), calls=%async_computation.9 | async-start | bytes 17039360 | tf_op jit(solution)/shard_map/all_gather | solution.py:56
Sparse Core Ops, SparseCore 0:
  9.8 28.1 all-gather.4
  45.0 19.4 all-gather.6
  285.7 205.2 all-gather.8
where the time goes:
time: 544 us; the launch traced here: 542 us
  waiting for transfers between devices  387 us (71%)
  local copies, waits for them, and re-layouts  48.7 us (9%)
  blocking collectives  35.9 us (7%)
  starting transfers between devices  25.4 us (5%)
  matrix products  22.9 us (4%)
  between operations  13.9 us (3%)
  other arithmetic  8.72 us (2%)
    all_gather x1, waiting for transfers between devices, gather_packed(): lines, at, outs = (lax.all_gather(flat, axis), 0, [])  187 us
    all_to_all x2, waiting for transfers between devices, sent_and_summed(): lax.all_to_all(pieces, axis, split_axis=0, concat_axis=0, tiled=True)  183 us
    all_to_all x2, starting transfers between devices, sent_and_summed(): lax.all_to_all(pieces, axis, split_axis=0, concat_axis=0, tiled=True)  21.6 us
    another operation x2, local copies, waits for them, and re-layouts, joined_along(): pieces.reshape(*lengths[:dim], lengths[dim] * lengths[dim + 1], *lengths[...  18.7 us
    all_to_all x1, blocking collectives, from_everyone(): lax.all_to_all(jnp.broadcast_to(shard[None], (devices, *shard.shape)), ax...  16.3 us
    all_gather x1, waiting for transfers between devices, in_one_piece(): lax.all_gather(both, axis, axis=dim, tiled=True)  16.1 us
    all_to_all x2, blocking collectives, sent_and_summed(): lax.all_to_all(pieces, axis, split_axis=0, concat_axis=0, tiled=True)  15.4 us
    all_gather x1, local copies, waits for them, and re-layouts, gather_packed(): lines, at, outs = (lax.all_gather(flat, axis), 0, [])  14.5 us
  transfers between devices with their start and end apart: 6, of which 4 were waited for; matrix products, arithmetic and copies ran while one was open for 5% of the time, Pallas kernels for 0%

commit v1 on v0

v1 whole, which is shorter than its diff:
```python
import functools

import jax
import jax.numpy as jnp
from jax import lax
from jax.experimental import pallas as pl
from jax.experimental.pallas import tpu as pltpu
from jax.sharding import PartitionSpec as P

MESH = pl.DeviceIdType.MESH
F32, BF16 = jnp.float32, jnp.bfloat16
NZ, NY, NX = 8, 4, 2
RINGS = {"y": NY, "z": NZ}
TOK, HALF, HID = 128, 1024, 2048
CH = 512
NCH = HID // CH
ROWS = 2 * HALF * HID // 128
TILE = 16
LANES = (("y", "z", 1, 19), ("z", "y", -1, 13), ("y", "z", -1, 19), ("z", "y", 1, 13))
PIECES = NY * NZ
RATE, LAG = 44000.0, 2.2


def hops(n, arm):
    return n // 2 if arm == 0 else n // 2 - 1


def planned():
    order, free, pending, joined = [], {}, [], {}
    now = 0.0

    def send(t, link, rows, what):
        start = max(t, free.get(link, 0.0))
        cost = rows * 256 / RATE * (2.0 if link == "x" else 1.0)
        free[link] = start + cost
        pending.append((start + cost + LAG, len(pending), what))

    def link_of(lane, phase, arm):
        first, second, sign, _ = LANES[lane]
        ring = first if phase in ("rs1", "ag1") else second
        way = sign if arm == 0 else -sign
        return (ring, -way if phase in ("rs1", "rs2") else way)

    def size(lane, phase):
        first, second, _, tiles = LANES[lane]
        piece = tiles * TILE
        return piece * RINGS[second] if phase in ("rs1", "ag1") else piece

    def ring_of(lane, phase):
        return RINGS[LANES[lane][0 if phase in ("rs1", "ag1") else 1]]

    def begin(t, lane, phase):
        order.append(("begin", lane, phase))
        if phase == "x":
            send(t, "x", size(lane, phase), (lane, "x", 0, 1))
            return
        joined[lane, phase] = 0
        for arm in (0, 1):
            send(t, link_of(lane, phase, arm), size(lane, phase), (lane, phase, arm, 1))

    for lane in range(len(LANES)):
        begin(now, lane, "rs1")
    after = {"rs1": "rs2", "rs2": "x", "x": "ag2", "ag2": "ag1", "ag1": None}
    while pending:
        pending.sort()
        at, _, (lane, phase, arm, k) = pending.pop(0)
        now = max(now, at) + 0.1
        last = phase == "x" or k == hops(ring_of(lane, phase), arm)
        if not last:
            order.append(("pass", lane, phase, arm, k))
            send(now, link_of(lane, phase, arm), size(lane, phase), (lane, phase, arm, k + 1))
            continue
        if phase != "x":
            joined[lane, phase] += 1
            if joined[lane, phase] < 2:
                continue
        order.append(("end", lane, phase))
        if after[phase]:
            begin(now, lane, after[phase])
    return order, now


ORDER, ESTIMATE = planned()


def transfers():
    table, rows = {}, 0
    for lane, (first, second, _, tiles) in enumerate(LANES):
        piece = tiles * TILE
        for phase, n, m in (("rs1", RINGS[first], piece * RINGS[second]), ("rs2", RINGS[second], piece)):
            for arm in (0, 1):
                for k in range(1, hops(n, arm) + 1):
                    table[lane, phase, arm, k] = (len(table), rows)
                    rows += m
        table[lane, "x", 0, 1] = (len(table), rows)
        rows += piece
        for phase, n in (("ag2", RINGS[second]), ("ag1", RINGS[first])):
            for arm in (0, 1):
                for k in range(1, hops(n, arm) + 1):
                    table[lane, phase, arm, k] = (len(table), None)
    return table, rows


TABLE, LANDING = transfers()


def dot(a, b, dims):
    return lax.dot_general(a, b, (dims, ((), ())), preferred_element_type=F32)


def body(in_ref, cot_ref, up_ref, down_ref, gin_ref, out_ref,
         x, c, xt, up, down, p_own, p_far, a_own, a_out, a_far, pre, sq, g, land, r, r_in,
         local_sem, xs, xr, ds, dr, gs, gr, ss, rs):
    rep, f, t = lax.axis_index("rep"), lax.axis_index("fs"), lax.axis_index("tp")
    xh = lax.rem(rep, NX)
    yz = rep // NX
    pos = {"y": lax.rem(yz, NY), "z": yz // NY}

    def at(ring, step):
        n = RINGS[ring]
        there = dict(pos)
        there[ring] = lax.rem(pos[ring] + step + n, n)
        return ((there["z"] * NY + there["y"]) * NX + xh, f, t)

    core = (rep, 1 - f, t)
    xpeer = (rep + 1 - 2 * xh, f, t)

    w_copies = [pltpu.make_async_copy(up_ref, up, local_sem.at[0]),
                pltpu.make_async_copy(down_ref, down, local_sem.at[1])]
    for w in w_copies:
        w.start()

    barrier = pltpu.get_barrier_semaphore()
    partners = [core, (rep, 0, 1 - t), (rep, 1, 1 - t), xpeer,
                at("y", 1), at("y", -1), at("z", 1), at("z", -1)]
    for who in partners:
        pl.semaphore_signal(barrier, inc=1, device_id=who, device_id_type=MESH)
    pl.semaphore_wait(barrier, len(partners))

    def remote(src, dst, send, recv, who):
        return pltpu.make_async_remote_copy(
            src_ref=src, dst_ref=dst, send_sem=send, recv_sem=recv, device_id=who, device_id_type=MESH)

    mine = pl.ds(pl.multiple_of(f * TOK, TOK), TOK)
    other = pl.ds(pl.multiple_of((1 - f) * TOK, TOK), TOK)
    home = f == t

    def across(i, src, dst):
        return remote(src, dst.at[mine], xs.at[i], xr.at[i, f], (rep, t, 1 - t))

    def beside(i, src, dst):
        return remote(src, dst.at[mine], xs.at[2 + i], xr.at[i, f], core)

    pairs = ((in_ref, x), (cot_ref, c))
    for i, (src, dst) in enumerate(pairs):
        across(i, src, dst).start()

        @pl.when(home)
        def _():
            dst[mine, :] = src[...]

        @pl.when(jnp.logical_not(home))
        def _():
            beside(i, src, dst).start()

    def landed(i, dst):
        @pl.when(jnp.logical_not(home))
        def _():
            remote(dst.at[mine], dst.at[mine], xs.at[i], xr.at[i, f], core).wait_recv()

        remote(dst.at[other], dst.at[other], xs.at[i], xr.at[i, 1 - f], core).wait_recv()

    def swap_p(i):
        return remote(p_own.at[i], p_far.at[i], ds.at[i], dr.at[i], core)

    def swap_a(i):
        return remote(a_out.at[i], a_far.at[i], ds.at[NCH + i], dr.at[NCH + i], core)

    landed(0, x)
    w_copies[0].wait()
    for i in range(NCH):
        p_own[i] = dot(x[...], up[:, i * CH:(i + 1) * CH], ((1,), (0,)))
        swap_p(i).start()
    xt[...] = x[...].T
    landed(1, c)
    w_copies[1].wait()
    for i in range(NCH):
        part = dot(c[...], down[i * CH:(i + 1) * CH, :], ((1,), (1,)))
        a_own[i] = part
        a_out[i] = part.astype(BF16)
        swap_a(i).start()
    for i in range(NCH):
        swap_p(i).wait_recv()
        swap_a(i).wait_recv()
        relu = jnp.maximum(p_own[i] + p_far[i], 0.0)
        sq[:, i * CH:(i + 1) * CH] = (relu * relu).astype(BF16)
        grad = a_own[i] + a_far[i].astype(F32)
        pre[:, i * CH:(i + 1) * CH] = (2.0 * relu * grad).astype(BF16)

    @pl.loop(0, NCH)
    def _(i):
        cols = pl.ds(pl.multiple_of(i * CH, CH), CH)
        part = dot(xt[...], pre[:, cols], ((1,), (0,)))
        for j in range(CH // 128):
            g[pl.ds(pl.multiple_of((i * (CH // 128) + j) * HALF, HALF), HALF), :] = (
                part[:, j * 128:(j + 1) * 128].astype(BF16))

    @pl.loop(0, NCH)
    def _(i):
        cols = pl.ds(pl.multiple_of(i * CH, CH), CH)
        part = dot(sq[:, cols].T, c[...], ((1,), (0,)))
        for j in range(HALF // 128):
            g[pl.ds(pl.multiple_of(ROWS // 2 + j * HID + i * CH, CH), CH), :] = (
                part[:, j * 128:(j + 1) * 128].astype(BF16))

    bases, base = [], 0
    for first, second, _, tiles in LANES:
        bases.append(base)
        base += tiles * TILE * PIECES
    started = {}

    def facts(lane, phase):
        first, second, sign, tiles = LANES[lane]
        piece = tiles * TILE
        whole = piece * RINGS[second]
        if phase in ("rs1", "ag1"):
            return first, sign, bases[lane], whole
        return second, sign, bases[lane] + pos[first] * whole, piece

    def chunk(lane, phase, step):
        ring, sign, start, rows = facts(lane, phase)
        n = RINGS[ring]
        there = lax.rem(pos[ring] + sign * step + n, n)
        return pl.multiple_of(start + there * rows, TILE), rows

    def send(lane, phase, arm, k):
        index, slot = TABLE[lane, phase, arm, k]
        ring, sign, _, rows = facts(lane, phase)
        way = sign if arm == 0 else -sign
        n = RINGS[ring]
        if phase == "x":
            begin, rows = chunk(lane, phase, 0)
            src, dst, who = g.at[pl.ds(begin, rows)], land.at[pl.ds(slot, rows)], xpeer
        elif slot is not None:
            left = hops(n, arm) - k + 1
            begin, rows = chunk(lane, phase, -left if arm == 0 else left)
            src, dst, who = g.at[pl.ds(begin, rows)], land.at[pl.ds(slot, rows)], at(ring, -way)
        else:
            gone = k - 1
            begin, rows = chunk(lane, phase, -gone if arm == 0 else gone)
            src = dst = out_ref.at[pl.ds(begin, rows)]
            who = at(ring, way)
        copy = remote(src, dst, ss.at[index], rs.at[index], who)
        copy.start()
        started[lane, phase, arm, k] = copy

    def add(target, begin, slots, rows, unit):
        @pl.loop(0, rows // unit)
        def _(i):
            here = pl.ds(pl.multiple_of(begin + i * unit, TILE), unit)
            total = g[here, :].astype(F32)
            for slot in slots:
                total += land[pl.ds(pl.multiple_of(slot + i * unit, TILE), unit), :].astype(F32)
            target[here, :] = total.astype(BF16)

    def run(order):
        for step in order:
            kind, lane, phase = step[:3]
            unit = LANES[lane][3] * TILE
            if kind == "begin":
                send(lane, phase, 0, 1)
                if phase != "x":
                    send(lane, phase, 1, 1)
            elif kind == "pass":
                arm, k = step[3:]
                started[lane, phase, arm, k].wait_recv()
                if phase in ("rs1", "rs2"):
                    left = hops(RINGS[facts(lane, phase)[0]], arm) - k
                    begin, rows = chunk(lane, phase, -left if arm == 0 else left)
                    add(g, begin, (TABLE[lane, phase, arm, k][1],), rows, unit)
                send(lane, phase, arm, k + 1)
            else:
                n = RINGS[facts(lane, phase)[0]]
                lasts = [(lane, phase, 0, 1)] if phase == "x" else [
                    (lane, phase, arm, hops(n, arm)) for arm in (0, 1)]
                for which in lasts:
                    started[which].wait_recv()
                slots = [TABLE[which][1] for which in lasts]
                begin, rows = chunk(lane, phase, 0)
                if phase in ("rs1", "rs2"):
                    add(g, begin, slots, rows, unit)
                elif phase == "x":
                    add(out_ref, begin, slots, rows, unit)

    opening = len(LANES)
    run(ORDER[:opening])

    @pl.loop(0, HALF // 256)
    def _(i):
        rows = pl.ds(pl.multiple_of(i * 256, 256), 256)
        r[:, rows] = dot(pre[...], up[rows, :], ((1,), (1,))).astype(BF16)

    def give(which, src, who):
        return remote(src, r_in.at[t], gs.at[which], gr.at[t], who)

    @pl.when(home)
    def _():
        give(1, r.at[other], core).start()
        r_in[t] = r[mine, :]

    @pl.when(jnp.logical_not(home))
    def _():
        give(0, r.at[pl.ds(0, TOK)], (rep, 0, 1 - t)).start()
        give(1, r.at[pl.ds(TOK, TOK)], (rep, 1, 1 - t)).start()

    half = len(ORDER) // 3
    run(ORDER[opening:half])

    @pl.when(jnp.logical_not(home))
    def _():
        remote(r_in.at[t], r_in.at[t], gs.at[0], gr.at[t], core).wait_recv()

    remote(r_in.at[1 - t], r_in.at[1 - t], gs.at[0], gr.at[1 - t], core).wait_recv()
    gin_ref[...] = (r_in[0].astype(F32) + r_in[1].astype(F32)).astype(BF16)

    run(ORDER[half:])

    for i, (src, dst) in enumerate(pairs):
        across(i, src, dst).wait_send()

        @pl.when(jnp.logical_not(home))
        def _():
            beside(i, src, dst).wait_send()
    for i in range(NCH):
        swap_p(i).wait_send()
        swap_a(i).wait_send()
    give(1, r.at[other], core).wait_send()

    @pl.when(jnp.logical_not(home))
    def _():
        give(0, r.at[other], core).wait_send()
    for copy in started.values():
        copy.wait_send()


def widen(g_ref, up_ref, down_ref):
    i = pl.program_id(0)

    @pl.when(i < 4)
    def _():
        for j in range(4):
            up_ref[:, j * 128:(j + 1) * 128] = g_ref[j * HALF:(j + 1) * HALF, :].astype(F32)

    @pl.when(i >= 4)
    def _():
        for j in range(2):
            down_ref[:, j * 128:(j + 1) * 128] = g_ref[j * HID:(j + 1) * HID, :].astype(F32)


def shards(inputs, cotangent, w_up, w_down):
    vmem, anywhere = pl.BlockSpec(memory_space=pltpu.VMEM), pl.BlockSpec(memory_space=pl.ANY)
    dma = pltpu.SemaphoreType.DMA
    grad_inputs, sums = pl.pallas_call(
        body,
        name="ffn_backward",
        out_shape=(jax.ShapeDtypeStruct((TOK, HALF), BF16), jax.ShapeDtypeStruct((ROWS, 128), BF16)),
        in_specs=[vmem, vmem, anywhere, anywhere],
        out_specs=(vmem, vmem),
        scratch_shapes=[
            pltpu.VMEM((2 * TOK, HALF), BF16), pltpu.VMEM((2 * TOK, HALF), BF16),
            pltpu.VMEM((HALF, 2 * TOK), BF16),
            pltpu.VMEM((HALF, HID), BF16), pltpu.VMEM((HID, HALF), BF16),
            pltpu.VMEM((NCH, 2 * TOK, CH), F32), pltpu.VMEM((NCH, 2 * TOK, CH), F32),
            pltpu.VMEM((NCH, 2 * TOK, CH), F32),
            pltpu.VMEM((NCH, 2 * TOK, CH), BF16), pltpu.VMEM((NCH, 2 * TOK, CH), BF16),
            pltpu.VMEM((2 * TOK, HID), BF16), pltpu.VMEM((2 * TOK, HID), BF16),
            pltpu.VMEM((ROWS, 128), BF16), pltpu.VMEM((LANDING, 128), BF16),
            pltpu.VMEM((2 * TOK, HALF), BF16), pltpu.VMEM((2, TOK, HALF), BF16),
            dma((2,)), dma((4,)), dma((2, 2)), dma((2 * NCH,)), dma((2 * NCH,)), dma((2,)), dma((2,)),
            dma((len(TABLE),)), dma((len(TABLE),)),
        ],
        compiler_params=pltpu.CompilerParams(
            collective_id=0, has_side_effects=True, vmem_limit_bytes=60 * 2**20),
    )(inputs, cotangent, w_up, w_down)
    grad_up, grad_down = pl.pallas_call(
        widen,
        name="widen",
        grid=(8,),
        out_shape=(jax.ShapeDtypeStruct((HALF, HID), F32), jax.ShapeDtypeStruct((HID, HALF), F32)),
        in_specs=[pl.BlockSpec((4096, 128), lambda i: (i, 0))],
        out_specs=(pl.BlockSpec((HALF, 512), lambda i: (0, jnp.minimum(i, 3))),
                   pl.BlockSpec((HID, 256), lambda i: (0, jnp.maximum(i - 4, 0)))),
    )(sums)
    return grad_inputs, grad_up, grad_down


def solution(mesh):
    return jax.shard_map(
        shards,
        mesh=mesh,
        in_specs=(P(("rep", "fs"), "tp"), P(("rep", "fs"), "tp"), P("fs", "tp"), P("tp", "fs")),
        out_specs=(P(("rep", "fs"), "tp"), P("fs", "tp"), P("tp", "fs")),
        check_vma=False,
    )
```

time: 544 us -> 191 us (0.35)
  the two profiles are of different devices: /device:TPU:8 before, /device:TPU:14 now
where the time goes in v1:
time: 191 us
  Pallas kernels  189 us (99%)
    pallas_call x1, Pallas kernels, shards(): pl.pallas_call(body, name='ffn_backward', out_shape=(jax.ShapeDtypeStruct...  178 us
    pallas_call x1, Pallas kernels, shards(): pl.pallas_call(widen, name='widen', grid=(8,), out_shape=(jax.ShapeDtypeS...  11.4 us

profile of v1, /device:TPU:14, one launch (start us, length us, event | category | flops | bytes accessed | tf_op | source)
XLA Modules:
  0.0 190.7 jit_solution(1047256789195787065)
XLA Ops:
  0.6 178.0 %ffn_backward.1 = (bf16[128,1024]{1,0:T(8,128)(2,1)}, bf16[32768,128]{1,0:T(8,128)(2,1)}) custom-call(bf16[128,1024]{1,0:T(8,128)(2,1)} %in_ref.1, bf16[128,1024]{1,0:T(8,128)(2,1)} %cot_ref.1, bf16[1024,2048]{1,0:T(8,128)(2,1)} %up_ref.1, bf16[2048,1024]{1,0:T(8,128)(2,1)} %down_ref.1), custom_call_target="tpu_custom_call" | custom-call | tf_op jit(solution)/shard_map/ffn_backward/pallas_call | solution.py:363
  178.6 0.0 copy-start
  178.6 11.4 %widen.1 = (f32[1024,2048]{1,0:T(8,128)}, f32[2048,1024]{1,0:T(8,128)}) custom-call(bf16[32768,128]{1,0:T(8,128)(2,1)} %get-tuple-element.8.g_ref), custom_call_target="tpu_custom_call" | custom-call | tf_op jit(solution)/shard_map/widen/pallas_call | solution.py:385
  190.0 0.0 copy-done
  190.0 0.7 copy.8
Async XLA Ops:
  178.6 11.4 %copy-start = (bf16[128,1024]{1,0:T(8,128)(2,1)S(1)}, bf16[128,1024]{1,0:T(8,128)(2,1)}, u32[]{:S(2)}) copy-start(bf16[128,1024]{1,0:T(8,128)(2,1)} %get-tuple-element.14) | copy-start | bytes 786436

commit v2 on v0

v2 whole, which is shorter than its diff:
```python
import functools

import jax
import jax.numpy as jnp
from jax import lax
from jax.experimental import pallas as pl
from jax.experimental.pallas import tpu as pltpu
from jax.sharding import PartitionSpec as P

MESH = pl.DeviceIdType.MESH
F32, BF16 = jnp.float32, jnp.bfloat16
NZ, NY, NX = 8, 4, 2
RINGS = {"y": NY, "z": NZ}
TOK, HALF, HID = 128, 1024, 2048
QUARTER = HID // 2
GRP = 2 * TOK
CH = 512
NCH = QUARTER // CH
ROWS = 2 * HALF * QUARTER // 128
TILE = 16
LANES = (("y", "z", 1, 5), ("z", "y", -1, 3), ("y", "z", -1, 5), ("z", "y", 1, 3)) * 2
STARTS = (0.0, 0.0, 1.0, 1.0, 2.5, 2.5, 3.5, 3.5)
PIECES = NY * NZ
RATE, LAG, WINDOW, WORK = 46000.0, 2.0, 3.0, 0.12
DEPTH = {"x": 0, "rs1": 1, "rs2": 1, "ag2": 2, "far2": 2, "ag1": 3, "far1": 3}
FIRST = ("rs1", "ag1", "far1")


def hops(n, arm):
    return n // 2 if arm == 0 else n // 2 - 1


def ring_of(lane, phase):
    return LANES[lane][0 if phase in FIRST else 1]


def length(lane, phase):
    piece = LANES[lane][3] * TILE
    return piece * RINGS[LANES[lane][1]] if phase in FIRST else piece


def last(lane, phase, arm, k):
    return phase == "x" or k == hops(RINGS[ring_of(lane, phase)], arm)


def planned():
    order, free, ready, flying, joined, now = [], {}, [], [], {}, 0.0

    def link_of(lane, phase, arm):
        if phase == "x":
            return "x"
        way = LANES[lane][2] if arm == 0 else -LANES[lane][2]
        return ring_of(lane, phase), -way if phase[:2] == "rs" else way

    def want(lane, phase, arm, k):
        rank = (DEPTH[phase], lane // 2, -k, len(order), len(ready))
        ready.append((rank, link_of(lane, phase, arm), (lane, phase, arm, k)))

    def begin(lane, phase):
        joined[lane, phase] = 0
        for arm in (0,) if phase == "x" else (0, 1):
            want(lane, phase, arm, 1)

    def issue():
        for item in sorted(ready):
            _, link, what = item
            start = max(now, free.get(link, 0.0))
            if start - now < WINDOW:
                ready.remove(item)
                cost = length(what[0], what[1]) * 256 / RATE * (2.0 if link == "x" else 1.0)
                free[link] = start + cost
                flying.append((start + cost + LAG, len(order), what))
                order.append(("send",) + what)

    todo = sorted((at, lane) for lane, at in enumerate(STARTS))
    while todo or flying:
        flying.sort()
        if todo and (not flying or todo[0][0] <= flying[0][0]):
            at, lane = todo.pop(0)
            now = max(now, at)
            order.append(("begin", lane))
            begin(lane, "rs1")
        else:
            at, _, (lane, phase, arm, k) = flying.pop(0)
            now = max(now, at) + WORK
            if not last(lane, phase, arm, k):
                order.append(("pass", lane, phase, arm, k))
                want(lane, phase, arm, k + 1)
            else:
                joined[lane, phase] += 1
                if phase == "x" or joined[lane, phase] == 2:
                    order.append(("end", lane, phase))
                    for after in {"rs1": ("rs2",), "rs2": ("x", "ag2"), "x": ("far2",),
                                  "ag2": ("ag1",), "far2": ("far1",)}.get(phase, ()):
                        begin(lane, after)
        issue()
        if ready and not flying and not todo:
            now = min(free[link] for _, link, _ in ready)
            issue()
    return order, now


ORDER, ESTIMATE = planned()


def transfers():
    table, rows = {}, 0
    for lane in range(len(LANES)):
        for phase in ("rs1", "rs2", "x", "ag2", "ag1", "far2", "far1"):
            for arm in (0,) if phase == "x" else (0, 1):
                for k in range(1, 2 if phase == "x" else hops(RINGS[ring_of(lane, phase)], arm) + 1):
                    lands = phase[:2] == "rs"
                    table[lane, phase, arm, k] = (len(table), rows if lands else None)
                    rows += length(lane, phase) if lands else 0
    return table, rows


TABLE, LANDING = transfers()


def dot(a, b, dims):
    return lax.dot_general(a, b, (dims, ((), ())), preferred_element_type=F32)


def body(in_ref, cot_ref, up_ref, down_ref, gin_ref, out_ref,
         x, c, xt, sqt, up, down, p_own, p_far, a_own, a_out, a_far, pre, sq, g, land, r, r_in,
         local_sem, xs, xr, fsem, ds, dr, gs, gr, ss, rs):
    rep, f, t = lax.axis_index("rep"), lax.axis_index("fs"), lax.axis_index("tp")
    xh = lax.rem(rep, NX)
    yz = rep // NX
    xpos = xh * 2 + t
    pos = {"y": lax.rem(yz, NY), "z": yz // NY}

    def at(ring, step):
        n = RINGS[ring]
        there = dict(pos)
        there[ring] = lax.rem(pos[ring] + step + n, n)
        return ((there["z"] * NY + there["y"]) * NX + xh, f, t)

    def along(step, who):
        there = lax.rem(xpos + step + 4, 4)
        return (yz * NX + there // 2, who, lax.rem(there, 2))

    core = (rep, 1 - f, t)
    xpeer = (yz * NX + 1 - xh, f, t)
    home = f == t
    away = jnp.logical_not(home)

    share = pl.ds(pl.multiple_of(xh * QUARTER, QUARTER), QUARTER)
    w_copies = [pltpu.make_async_copy(up_ref.at[:, share], up, local_sem.at[0]),
                pltpu.make_async_copy(down_ref.at[share, :], down, local_sem.at[1])]
    for w in w_copies:
        w.start()

    barrier = pltpu.get_barrier_semaphore()
    partners = [core] + [along(step, who) for step in (1, -1, 2) for who in (0, 1)] + [
        at("y", 1), at("y", -1), at("z", 1), at("z", -1)]
    for who in partners:
        pl.semaphore_signal(barrier, inc=1, device_id=who, device_id_type=MESH)
    pl.semaphore_wait(barrier, len(partners))

    def remote(src, dst, send, recv, who):
        return pltpu.make_async_remote_copy(
            src_ref=src, dst_ref=dst, send_sem=send, recv_sem=recv, device_id=who, device_id_type=MESH)

    def block(group, who):
        return pl.ds(pl.multiple_of((group * 2 + who) * TOK, TOK), TOK)

    pairs = ((in_ref, x), (cot_ref, c))

    def across(i, way):
        src, dst = pairs[i]
        group = t if way == 1 else 1 - t
        return remote(src, dst.at[block(group, f)], xs.at[i, 0 if way == 1 else 1],
                      xr.at[i, group * 2 + f], along(way, t))

    def beside(i):
        src, dst = pairs[i]
        return remote(src, dst.at[block(0, f)], xs.at[i, 2], xr.at[i, f], core)

    def onward(i, way):
        _, dst = pairs[i]
        group, who = (1 - t, 0) if way == 1 else (t, 1)
        return remote(dst.at[block(group, who)], dst.at[block(1, who)], fsem.at[i, who],
                      xr.at[i, 2 + who], along(way, f))

    def landed(i, group, who):
        _, dst = pairs[i]
        there = dst.at[block(group, who)]
        remote(there, there, xs.at[i, 0], xr.at[i, group * 2 + who], core).wait_recv()

    for i in (0, 1):
        across(i, 1).start()
        across(i, -1).start()
        src, dst = pairs[i]

        @pl.when(home)
        def _():
            dst[block(0, f), :] = src[...]

        @pl.when(away)
        def _():
            beside(i).start()

    def pass_on(i):
        @pl.when(away)
        def _():
            landed(i, 1 - t, 0)
            onward(i, 1).start()
            landed(i, t, 1)
            onward(i, -1).start()

    def arrive(i, group):
        if group == 0:
            @pl.when(home)
            def _():
                landed(i, 0, 1 - f)
        else:
            @pl.when(home)
            def _():
                landed(i, 1, 0)
                landed(i, 1, 1)

        @pl.when(away)
        def _():
            landed(i, group, jnp.where(group == t, 0, 1))

    def swap_p(i):
        return remote(p_own.at[i], p_far.at[i], ds.at[i], dr.at[i], core)

    def swap_a(i):
        return remote(a_out.at[i], a_far.at[i], ds.at[2 * NCH + i], dr.at[2 * NCH + i], core)

    def first_product(group):
        arrive(0, group)
        here = pl.ds(group * GRP, GRP)
        for j in range(NCH):
            i = group * NCH + j
            p_own[i] = dot(x[here, :], up[:, j * CH:(j + 1) * CH], ((1,), (0,)))
            swap_p(i).start()
        xt[:, here] = x[here, :].T

    def second_product(group):
        arrive(1, group)
        here = pl.ds(group * GRP, GRP)
        for j in range(NCH):
            i = group * NCH + j
            part = dot(c[here, :], down[j * CH:(j + 1) * CH, :], ((1,), (1,)))
            a_own[i] = part
            a_out[i] = part.astype(BF16)
            swap_a(i).start()

    pass_on(0)
    for w in w_copies:
        w.wait()
    first_product(0)
    pass_on(1)
    second_product(0)
    first_product(1)
    second_product(1)

    def activations(j):
        cols = slice(j * CH, (j + 1) * CH)
        for group in (0, 1):
            i = group * NCH + j
            swap_p(i).wait_recv()
            swap_a(i).wait_recv()
            here = slice(group * GRP, (group + 1) * GRP)
            relu = jnp.maximum(p_own[i] + p_far[i], 0.0)
            sq[here, cols] = (relu * relu).astype(BF16)
            grad = a_own[i] + a_far[i].astype(F32)
            pre[here, cols] = (2.0 * relu * grad).astype(BF16)

    def local_up(j):
        activations(j)
        part = dot(xt[...], pre[:, j * CH:(j + 1) * CH], ((1,), (0,)))
        for k in range(CH // 128):
            g[(j * 4 + k) * HALF:(j * 4 + k + 1) * HALF, :] = part[:, k * 128:(k + 1) * 128].astype(BF16)

    def local_down(j):
        if j == 0:
            sqt[...] = sq[...].T
        part = dot(sqt[...], c[:, j * CH:(j + 1) * CH], ((1,), (0,)))
        for k in range(CH // 128):
            g[(8 + j * 4 + k) * HALF:(9 + j * 4 + k) * HALF, :] = part[:, k * 128:(k + 1) * 128].astype(BF16)

    def inputs_part(j):
        rows = slice(j * 256, (j + 1) * 256)
        r[:, rows] = dot(pre[...], up[rows, :], ((1,), (1,))).astype(BF16)

    def give(group, who):
        there = jnp.where(group == 0, xh, 1 - xh)
        return remote(r.at[block(group, who)], r_in.at[xpos], gs.at[group, who], gr.at[xpos],
                      (yz * NX + there, who, f))

    def give_all():
        @pl.when(home)
        def _():
            give(0, 1 - f).start()
            r_in[xpos] = r[block(0, f), :]

        @pl.when(away)
        def _():
            give(0, f).start()
            give(0, 1 - f).start()

        give(1, 0).start()
        give(1, 1).start()

    def inputs_sum():
        def came(k):
            there = r_in.at[k]
            remote(there, there, gs.at[0, 0], gr.at[k], core).wait_recv()

        @pl.when(away)
        def _():
            came(xpos)

        for step in (1, 2, 3):
            came(lax.rem(xpos + step, 4))
        total = r_in[0].astype(F32)
        for k in range(1, 4):
            total += r_in[k].astype(F32)
        gin_ref[...] = total.astype(BF16)

    bases, base = [], 0
    for lane in range(len(LANES)):
        bases.append(base)
        base += LANES[lane][3] * TILE * PIECES
    started = {}

    def chunk(lane, phase, step):
        ring = ring_of(lane, phase)
        rows = length(lane, phase)
        start = bases[lane]
        if phase not in FIRST:
            start += pos[LANES[lane][0]] * length(lane, "rs1")
        if phase[:2] == "ag" or phase == "x":
            start += xh * ROWS
        elif phase[:3] == "far":
            start += (1 - xh) * ROWS
        n = RINGS[ring]
        there = lax.rem(pos[ring] + LANES[lane][2] * step + n, n)
        return pl.multiple_of(start + there * rows, TILE), rows

    def send(lane, phase, arm, k):
        index, slot = TABLE[lane, phase, arm, k]
        ring = ring_of(lane, phase)
        way = LANES[lane][2] if arm == 0 else -LANES[lane][2]
        if phase == "x":
            begin, rows = chunk(lane, phase, 0)
            src = dst = out_ref.at[pl.ds(begin, rows)]
            who = xpeer
        elif slot is not None:
            left = hops(RINGS[ring], arm) - k + 1
            begin, rows = chunk(lane, phase, -left if arm == 0 else left)
            src, dst, who = g.at[pl.ds(begin, rows)], land.at[pl.ds(slot, rows)], at(ring, -way)
        else:
            begin, rows = chunk(lane, phase, 1 - k if arm == 0 else k - 1)
            src = dst = out_ref.at[pl.ds(begin, rows)]
            who = at(ring, way)
        copy = remote(src, dst, ss.at[index], rs.at[index], who)
        copy.start()
        started[lane, phase, arm, k] = copy

    def add(target, shift, begin, slots, rows, unit):
        @pl.loop(0, rows // unit)
        def _(i):
            here = pl.multiple_of(begin + i * unit, TILE)
            total = g[pl.ds(here, unit), :].astype(F32)
            for slot in slots:
                total += land[pl.ds(pl.multiple_of(slot + i * unit, TILE), unit), :].astype(F32)
            target[pl.ds(pl.multiple_of(here + shift, TILE), unit), :] = total.astype(BF16)

    aside = [functools.partial(inputs_part, j) for j in range(4)] + [give_all]
    begun = 0
    for count, step in enumerate(ORDER):
        kind, lane = step[:2]
        unit = LANES[lane][3] * TILE
        if kind == "begin":
            begun += 1
            if lane % 2 == 0:
                (local_up, local_down)[lane // 4](lane // 2 % 2)
        elif kind == "send":
            send(*step[1:])
        elif kind == "pass":
            phase, arm, k = step[2:]
            started[lane, phase, arm, k].wait_recv()
            if phase[:2] == "rs":
                left = hops(RINGS[ring_of(lane, phase)], arm) - k
                begin, rows = chunk(lane, phase, -left if arm == 0 else left)
                add(g, 0, begin, (TABLE[lane, phase, arm, k][1],), rows, unit)
            if begun == len(LANES) and aside:
                aside.pop(0)()
        else:
            phase = step[2]
            n = RINGS[ring_of(lane, phase)]
            ends = [(lane, phase, 0, 1)] if phase == "x" else [
                (lane, phase, arm, hops(n, arm)) for arm in (0, 1)]
            for which in ends:
                started[which].wait_recv()
            if phase[:2] == "rs":
                begin, rows = chunk(lane, phase, 0)
                into, shift = (g, 0) if phase == "rs1" else (out_ref, xh * ROWS)
                add(into, shift, begin, [TABLE[which][1] for which in ends], rows, unit)
        if count == len(ORDER) * 3 // 5:
            inputs_sum()

    for i in (0, 1):
        across(i, 1).wait_send()
        across(i, -1).wait_send()

        @pl.when(away)
        def _():
            beside(i).wait_send()
            onward(i, 1).wait_send()
            onward(i, -1).wait_send()
    for i in range(2 * NCH):
        swap_p(i).wait_send()
        swap_a(i).wait_send()

    give(0, 1 - f).wait_send()
    give(1, 0).wait_send()
    give(1, 1).wait_send()

    @pl.when(away)
    def _():
        give(0, f).wait_send()
    for copy in started.values():
        copy.wait_send()


def widen(g_ref, up_ref, down_ref):
    i = lax.rem(pl.program_id(0), 4)

    @pl.when(i < 2)
    def _():
        for j in range(4):
            up_ref[:, j * 128:(j + 1) * 128] = g_ref[j * HALF:(j + 1) * HALF, :].astype(F32)

    @pl.when(i >= 2)
    def _():
        for j in range(4):
            down_ref[:, j * 128:(j + 1) * 128] = g_ref[j * HALF:(j + 1) * HALF, :].astype(F32)


def shards(inputs, cotangent, w_up, w_down):
    vmem, anywhere = pl.BlockSpec(memory_space=pltpu.VMEM), pl.BlockSpec(memory_space=pl.ANY)
    dma = pltpu.SemaphoreType.DMA
    grad_inputs, sums = pl.pallas_call(
        body,
        name="ffn_backward",
        out_shape=(jax.ShapeDtypeStruct((TOK, HALF), BF16), jax.ShapeDtypeStruct((2 * ROWS, 128), BF16)),
        in_specs=[vmem, vmem, anywhere, anywhere],
        out_specs=(vmem, vmem),
        scratch_shapes=[
            pltpu.VMEM((2 * GRP, HALF), BF16), pltpu.VMEM((2 * GRP, HALF), BF16),
            pltpu.VMEM((HALF, 2 * GRP), BF16), pltpu.VMEM((QUARTER, 2 * GRP), BF16),
            pltpu.VMEM((HALF, QUARTER), BF16), pltpu.VMEM((QUARTER, HALF), BF16),
            pltpu.VMEM((2 * NCH, GRP, CH), F32), pltpu.VMEM((2 * NCH, GRP, CH), F32),
            pltpu.VMEM((2 * NCH, GRP, CH), F32),
            pltpu.VMEM((2 * NCH, GRP, CH), BF16), pltpu.VMEM((2 * NCH, GRP, CH), BF16),
            pltpu.VMEM((2 * GRP, QUARTER), BF16), pltpu.VMEM((2 * GRP, QUARTER), BF16),
            pltpu.VMEM((ROWS, 128), BF16), pltpu.VMEM((LANDING, 128), BF16),
            pltpu.VMEM((2 * GRP, HALF), BF16), pltpu.VMEM((4, TOK, HALF), BF16),
            dma((2,)), dma((2, 3)), dma((2, 4)), dma((2, 2)), dma((4 * NCH,)), dma((4 * NCH,)),
            dma((2, 2)), dma((4,)), dma((len(TABLE),)), dma((len(TABLE),)),
        ],
        compiler_params=pltpu.CompilerParams(
            collective_id=0, has_side_effects=True, vmem_limit_bytes=60 * 2**20),
    )(inputs, cotangent, w_up, w_down)
    grad_up, grad_down = pl.pallas_call(
        widen,
        name="widen",
        grid=(8,),
        out_shape=(jax.ShapeDtypeStruct((HALF, HID), F32), jax.ShapeDtypeStruct((HID, HALF), F32)),
        in_specs=[pl.BlockSpec((4096, 128), lambda i: (i, 0))],
        out_specs=(
            pl.BlockSpec((HALF, 512), lambda i: (0, i // 4 * 2 + jnp.minimum(lax.rem(i, 4), 1))),
            pl.BlockSpec((HALF, 512), lambda i: (i // 4, jnp.maximum(lax.rem(i, 4) - 2, 0)))),
    )(sums)
    return grad_inputs, grad_up, grad_down


def solution(mesh):
    return jax.shard_map(
        shards,
        mesh=mesh,
        in_specs=(P(("rep", "fs"), "tp"), P(("rep", "fs"), "tp"), P("fs", "tp"), P("tp", "fs")),
        out_specs=(P(("rep", "fs"), "tp"), P("fs", "tp"), P("tp", "fs")),
        check_vma=False,
    )
```

time: 544 us -> 147 us (0.27)
  waiting for transfers between devices: 387 us -> 0 us
  Pallas kernels: 0 us -> 145 us
  local copies, waits for them, and re-layouts: 48.7 us -> 0.71 us
  blocking collectives: 35.9 us -> 0 us
  starting transfers between devices: 25.4 us -> 0 us
  matrix products: 22.9 us -> 0 us
  between operations: 13.9 us -> 0.65 us
  other arithmetic: 8.72 us -> 0 us
    all_gather x3 -> x0, waiting for transfers between devices: 203 us -> none  [the longest x1 187 us: gather_packed(): lines, at, outs = (lax.all_gather(flat, axis), 0, [])]
    all_to_all x3 -> x0, waiting for transfers between devices: 183 us -> none  [the longest x2 183 us: sent_and_summed(): lax.all_to_all(pieces, axis, split_axis=0, concat_axis=0, tiled=True)]
    pallas_call x0 -> x2, Pallas kernels: none -> 145 us  [the longest x1 133 us: shards(): pl.pallas_call(body, name='ffn_backward', out_shape=(jax.ShapeDtypeStruct...]
    all_to_all x4 -> x0, blocking collectives: 35.9 us -> none  [the longest x1 16.3 us: from_everyone(): lax.all_to_all(jnp.broadcast_to(shard[None], (devices, *shard.shape)), ax...]
    all_to_all x3 -> x0, starting transfers between devices: 25.1 us -> none  [the longest x2 21.6 us: sent_and_summed(): lax.all_to_all(pieces, axis, split_axis=0, concat_axis=0, tiled=True)]
    dot_general x5 -> x0, matrix products: 22.9 us -> none  [the longest x2 10.1 us: contract_cols(): lax.dot_general(left, right, (((1,), (1,)), ((), ())), preferred_element_...]
    another operation x2 -> x0, local copies, waits for them, and re-layouts: 18.7 us -> none  [joined_along(): pieces.reshape(*lengths[:dim], lengths[dim] * lengths[dim + 1], *lengths[...]
    all_gather x1 -> x0, local copies, waits for them, and re-layouts: 14.5 us -> none  [gather_packed(): lines, at, outs = (lax.all_gather(flat, axis), 0, [])]
  transfers between devices with their start and end apart: 6 -> 0, of which waited for: 4 -> 0; matrix products, arithmetic and copies ran while one was open for 5% -> 0% of each run, Pallas kernels for 0% -> 0%
where the time goes in v2:
time: 147 us; the launch traced here: 146 us
  Pallas kernels  145 us (99%)
    pallas_call x1, Pallas kernels, shards(): pl.pallas_call(body, name='ffn_backward', out_shape=(jax.ShapeDtypeStruct...  133 us
    pallas_call x1, Pallas kernels, shards(): pl.pallas_call(widen, name='widen', grid=(8,), out_shape=(jax.ShapeDtypeS...  11.6 us

profile of v2, /device:TPU:8, one launch (start us, length us, event | category | flops | bytes accessed | tf_op | source)
XLA Modules:
  0.0 146.3 jit_solution(758543405107009293)
XLA Ops:
  0.6 133.3 %ffn_backward.1 = (bf16[128,1024]{1,0:T(8,128)(2,1)}, bf16[32768,128]{1,0:T(8,128)(2,1)}) custom-call(bf16[128,1024]{1,0:T(8,128)(2,1)} %in_ref.1, bf16[128,1024]{1,0:T(8,128)(2,1)} %cot_ref.1, bf16[1024,2048]{1,0:T(8,128)(2,1)} %up_ref.1, bf16[2048,1024]{1,0:T(8,128)(2,1)} %down_ref.1), custom_call_target="tpu_custom_call" | custom-call | tf_op jit(solution)/shard_map/ffn_backward/pallas_call | solution.py:450
  134.0 0.0 copy-start
  134.0 11.6 %widen.1 = (f32[1024,2048]{1,0:T(8,128)}, f32[2048,1024]{1,0:T(8,128)}) custom-call(bf16[32768,128]{1,0:T(8,128)(2,1)} %get-tuple-element.8.g_ref), custom_call_target="tpu_custom_call" | custom-call | tf_op jit(solution)/shard_map/widen/pallas_call | solution.py:472
  145.6 0.0 copy-done
  145.6 0.7 copy.8
Async XLA Ops:
  134.0 11.6 %copy-start = (bf16[128,1024]{1,0:T(8,128)(2,1)S(1)}, bf16[128,1024]{1,0:T(8,128)(2,1)}, u32[]{:S(2)}) copy-start(bf16[128,1024]{1,0:T(8,128)(2,1)} %get-tuple-element.14) | copy-start | bytes 786436

commit v3 on v2

--- a/solution.py
+++ b/solution.py
@@ -1,4 +1,5 @@
 import functools
+import heapq
 
 import jax
 import jax.numpy as jnp
@@ -18,11 +19,21 @@
 NCH = QUARTER // CH
 ROWS = 2 * HALF * QUARTER // 128
 TILE = 16
-LANES = (("y", "z", 1, 5), ("z", "y", -1, 3), ("y", "z", -1, 5), ("z", "y", 1, 3)) * 2
-STARTS = (0.0, 0.0, 1.0, 1.0, 2.5, 2.5, 3.5, 3.5)
+A, B = ("y", "z"), ("z", "y")
+LANES = ((*A, 1, 3), (*B, -1, 2), (*A, -1, 3), (*B, 1, 2), (*A, 1, 3), (*B, -1, 2), (*A, -1, 3),
+         (*A, 1, 3), (*B, 1, 2), (*A, -1, 3), (*B, -1, 2), (*A, 1, 1), (*B, 1, 2), (*A, -1, 1))
+UPTO = tuple(sum(lane[3] for lane in LANES[:i + 1]) for i in range(len(LANES)))
+STARTS = tuple(2.4 * tiles / 32 for tiles in UPTO)
 PIECES = NY * NZ
-RATE, LAG, WINDOW, WORK = 46000.0, 2.0, 3.0, 0.12
-DEPTH = {"x": 0, "rs1": 1, "rs2": 1, "ag2": 2, "far2": 2, "ag1": 3, "far1": 3}
+RATE, LAG, WINDOW, WORK = 46000.0, 2.0, 1.6, 0.12
+RANKS = {
+    "rs1": (8, 39, 32, 19, 44, 56, 71, 34, 12, 58, 65, 47, 29, 68),
+    "rs2": (16, 70, 64, 91, 37, 17, 83, 21, 78, 72, 95, 84, 80, 87),
+    "x": (46, 59, 52, 74, 51, 3, 48, 0, 61, 50, 18, 88, 41, 9),
+    "ag2": (35, 24, 40, 62, 13, 94, 77, 55, 57, 67, 85, 66, 27, 43),
+    "ag1": (42, 97, 75, 38, 10, 14, 11, 2, 81, 86, 54, 53, 79, 45),
+    "far2": (4, 33, 22, 23, 31, 30, 73, 63, 82, 5, 49, 69, 28, 60),
+    "far1": (15, 89, 1, 76, 25, 90, 92, 7, 96, 26, 6, 36, 20, 93)}
 FIRST = ("rs1", "ag1", "far1")
 
 
@@ -44,7 +55,7 @@
 
 
 def planned():
-    order, free, ready, flying, joined, now = [], {}, [], [], {}, 0.0
+    order, free, ready, flying, joined, now, count = [], {}, {}, [], {}, 0.0, 0
 
     def link_of(lane, phase, arm):
         if phase == "x":
@@ -53,8 +64,10 @@
         return ring_of(lane, phase), -way if phase[:2] == "rs" else way
 
     def want(lane, phase, arm, k):
-        rank = (DEPTH[phase], lane // 2, -k, len(order), len(ready))
-        ready.append((rank, link_of(lane, phase, arm), (lane, phase, arm, k)))
+        nonlocal count
+        count += 1
+        line = ready.setdefault(link_of(lane, phase, arm), [])
+        heapq.heappush(line, (RANKS[phase][lane], -k, count, (lane, phase, arm, k)))
 
     def begin(lane, phase):
         joined[lane, phase] = 0
@@ -62,26 +75,25 @@
             want(lane, phase, arm, 1)
 
     def issue():
-        for item in sorted(ready):
-            _, link, what = item
-            start = max(now, free.get(link, 0.0))
-            if start - now < WINDOW:
-                ready.remove(item)
-                cost = length(what[0], what[1]) * 256 / RATE * (2.0 if link == "x" else 1.0)
-                free[link] = start + cost
-                flying.append((start + cost + LAG, len(order), what))
+        nonlocal count
+        for link, line in ready.items():
+            while line and max(now, free.get(link, 0.0)) - now < WINDOW:
+                what = heapq.heappop(line)[3]
+                cost = length(what[0], what[1]) * 256 * (2 if link == "x" else 1) / RATE
+                free[link] = max(now, free.get(link, 0.0)) + cost
+                count += 1
+                heapq.heappush(flying, (free[link] + LAG, count, what))
                 order.append(("send",) + what)
 
     todo = sorted((at, lane) for lane, at in enumerate(STARTS))
     while todo or flying:
-        flying.sort()
         if todo and (not flying or todo[0][0] <= flying[0][0]):
             at, lane = todo.pop(0)
             now = max(now, at)
             order.append(("begin", lane))
             begin(lane, "rs1")
         else:
-            at, _, (lane, phase, arm, k) = flying.pop(0)
+            at, _, (lane, phase, arm, k) = heapq.heappop(flying)
             now = max(now, at) + WORK
             if not last(lane, phase, arm, k):
                 order.append(("pass", lane, phase, arm, k))
@@ -94,8 +106,8 @@
                                   "ag2": ("ag1",), "far2": ("far1",)}.get(phase, ()):
                         begin(lane, after)
         issue()
-        if ready and not flying and not todo:
-            now = min(free[link] for _, link, _ in ready)
+        if not flying and not todo and any(ready.values()):
+            now = min(free[link] for link, line in ready.items() if line)
             issue()
     return order, now
 
@@ -122,9 +134,9 @@
     return lax.dot_general(a, b, (dims, ((), ())), preferred_element_type=F32)
 
 
-def body(in_ref, cot_ref, up_ref, down_ref, gin_ref, out_ref,
-         x, c, xt, sqt, up, down, p_own, p_far, a_own, a_out, a_far, pre, sq, g, land, r, r_in,
-         local_sem, xs, xr, fsem, ds, dr, gs, gr, ss, rs):
+def body(in_ref, cot_ref, up_ref, down_ref, gin_ref, sums_ref,
+         in_v, cot_v, out_ref, x, c, xt, sqt, up, down, p_own, p_far, a_own, a_out, a_far, pre, sq, g, land, r, r_in,
+         local_sem, xs, xr, fsem, ds, dr, gs, gr, ss, rs, os):
     rep, f, t = lax.axis_index("rep"), lax.axis_index("fs"), lax.axis_index("tp")
     xh = lax.rem(rep, NX)
     yz = rep // NX
@@ -149,8 +161,10 @@
     share = pl.ds(pl.multiple_of(xh * QUARTER, QUARTER), QUARTER)
     w_copies = [pltpu.make_async_copy(up_ref.at[:, share], up, local_sem.at[0]),
                 pltpu.make_async_copy(down_ref.at[share, :], down, local_sem.at[1])]
-    for w in w_copies:
-        w.start()
+    t_copies = [pltpu.make_async_copy(in_ref, in_v, local_sem.at[2]),
+                pltpu.make_async_copy(cot_ref, cot_v, local_sem.at[3])]
+    for copy in t_copies + w_copies:
+        copy.start()
 
     barrier = pltpu.get_barrier_semaphore()
     partners = [core] + [along(step, who) for step in (1, -1, 2) for who in (0, 1)] + [
@@ -166,7 +180,7 @@
     def block(group, who):
         return pl.ds(pl.multiple_of((group * 2 + who) * TOK, TOK), TOK)
 
-    pairs = ((in_ref, x), (cot_ref, c))
+    pairs = ((in_v, x), (cot_v, c))
 
     def across(i, way):
         src, dst = pairs[i]
@@ -190,6 +204,7 @@
         remote(there, there, xs.at[i, 0], xr.at[i, group * 2 + who], core).wait_recv()
 
     for i in (0, 1):
+        t_copies[i].wait()
         across(i, 1).start()
         across(i, -1).start()
         src, dst = pairs[i]
@@ -363,7 +378,9 @@
         copy.start()
         started[lane, phase, arm, k] = copy
 
-    def add(target, shift, begin, slots, rows, unit):
+    def add(target, shift, begin, slots, rows):
+        unit = max(u for u in range(TILE, 193, TILE) if rows % u == 0)
+
         @pl.loop(0, rows // unit)
         def _(i):
             here = pl.multiple_of(begin + i * unit, TILE)
@@ -373,14 +390,15 @@
             target[pl.ds(pl.multiple_of(here + shift, TILE), unit), :] = total.astype(BF16)
 
     aside = [functools.partial(inputs_part, j) for j in range(4)] + [give_all]
-    begun = 0
+    leaving = []
+    begun = chunks = 0
     for count, step in enumerate(ORDER):
         kind, lane = step[:2]
-        unit = LANES[lane][3] * TILE
         if kind == "begin":
             begun += 1
-            if lane % 2 == 0:
-                (local_up, local_down)[lane // 4](lane // 2 % 2)
+            while chunks * 8 < UPTO[lane]:
+                (local_up, local_down)[chunks // 2](chunks % 2)
+                chunks += 1
         elif kind == "send":
             send(*step[1:])
         elif kind == "pass":
@@ -389,7 +407,7 @@
             if phase[:2] == "rs":
                 left = hops(RINGS[ring_of(lane, phase)], arm) - k
                 begin, rows = chunk(lane, phase, -left if arm == 0 else left)
-                add(g, 0, begin, (TABLE[lane, phase, arm, k][1],), rows, unit)
+                add(g, 0, begin, (TABLE[lane, phase, arm, k][1],), rows)
             if begun == len(LANES) and aside:
                 aside.pop(0)()
         else:
@@ -402,7 +420,13 @@
             if phase[:2] == "rs":
                 begin, rows = chunk(lane, phase, 0)
                 into, shift = (g, 0) if phase == "rs1" else (out_ref, xh * ROWS)
-                add(into, shift, begin, [TABLE[which][1] for which in ends], rows, unit)
+                add(into, shift, begin, [TABLE[which][1] for which in ends], rows)
+            elif phase in ("ag1", "far1"):
+                half = xh if phase == "ag1" else 1 - xh
+                there = pl.ds(pl.multiple_of(half * ROWS + bases[lane], TILE), LANES[lane][3] * TILE * PIECES)
+                leaving.append(pltpu.make_async_copy(
+                    out_ref.at[there], sums_ref.at[there], os.at[len(leaving)]))
+                leaving[-1].start()
         if count == len(ORDER) * 3 // 5:
             inputs_sum()
 
@@ -428,32 +452,56 @@
         give(0, f).wait_send()
     for copy in started.values():
         copy.wait_send()
-
-
-def widen(g_ref, up_ref, down_ref):
-    i = lax.rem(pl.program_id(0), 4)
-
-    @pl.when(i < 2)
-    def _():
-        for j in range(4):
-            up_ref[:, j * 128:(j + 1) * 128] = g_ref[j * HALF:(j + 1) * HALF, :].astype(F32)
-
-    @pl.when(i >= 2)
-    def _():
-        for j in range(4):
-            down_ref[:, j * 128:(j + 1) * 128] = g_ref[j * HALF:(j + 1) * HALF, :].astype(F32)
+    for copy in leaving:
+        copy.wait()
+
+
+PARTS = 8
+
+
+def widen(gin_ref, sums_ref, gin_out, up_out, down_out, gin, narrow, wide, sem, read, write):
+    through = pltpu.make_async_copy(gin_ref, gin, sem.at[0])
+    through.start()
+    rows, columns = 2 * ROWS // PARTS, 2 * ROWS // PARTS // HALF
+    reads = []
+    for i in range(PARTS):
+        there = pl.ds(i * rows, rows)
+        reads.append(pltpu.make_async_copy(sums_ref.at[there], narrow.at[there], read.at[i]))
+        reads[i].start()
+    writes = []
+    for i in range(PARTS):
+        reads[i].wait()
+        first = i * columns
+        for j in range(first, first + columns):
+            wide[:, j * 128:(j + 1) * 128] = narrow[j * HALF:(j + 1) * HALF, :].astype(F32)
+        half, column = first // 16, first % 16
+        if column < 8:
+            there = up_out.at[:, pl.ds(half * QUARTER + column * 128, columns * 128)]
+        else:
+            there = down_out.at[pl.ds(half * QUARTER, QUARTER), pl.ds((column - 8) * 128, columns * 128)]
+        writes.append(pltpu.make_async_copy(wide.at[:, pl.ds(first * 128, columns * 128)], there, write.at[i]))
+        writes[i].start()
+        if i == 0:
+            through.wait()
+            back = pltpu.make_async_copy(gin, gin_out, sem.at[1])
+            back.start()
+    back.wait()
+    for copy in writes:
+        copy.wait()
 
 
 def shards(inputs, cotangent, w_up, w_down):
     vmem, anywhere = pl.BlockSpec(memory_space=pltpu.VMEM), pl.BlockSpec(memory_space=pl.ANY)
+    gin_shape = jax.ShapeDtypeStruct((TOK, HALF), BF16)
     dma = pltpu.SemaphoreType.DMA
     grad_inputs, sums = pl.pallas_call(
         body,
         name="ffn_backward",
-        out_shape=(jax.ShapeDtypeStruct((TOK, HALF), BF16), jax.ShapeDtypeStruct((2 * ROWS, 128), BF16)),
-        in_specs=[vmem, vmem, anywhere, anywhere],
-        out_specs=(vmem, vmem),
+        out_shape=(gin_shape, jax.ShapeDtypeStruct((2 * ROWS, 128), BF16)),
+        in_specs=[anywhere] * 4,
+        out_specs=(vmem, anywhere),
         scratch_shapes=[
+            pltpu.VMEM((TOK, HALF), BF16), pltpu.VMEM((TOK, HALF), BF16), pltpu.VMEM((2 * ROWS, 128), BF16),
             pltpu.VMEM((2 * GRP, HALF), BF16), pltpu.VMEM((2 * GRP, HALF), BF16),
             pltpu.VMEM((HALF, 2 * GRP), BF16), pltpu.VMEM((QUARTER, 2 * GRP), BF16),
             pltpu.VMEM((HALF, QUARTER), BF16), pltpu.VMEM((QUARTER, HALF), BF16),
@@ -463,23 +511,25 @@
             pltpu.VMEM((2 * GRP, QUARTER), BF16), pltpu.VMEM((2 * GRP, QUARTER), BF16),
             pltpu.VMEM((ROWS, 128), BF16), pltpu.VMEM((LANDING, 128), BF16),
             pltpu.VMEM((2 * GRP, HALF), BF16), pltpu.VMEM((4, TOK, HALF), BF16),
-            dma((2,)), dma((2, 3)), dma((2, 4)), dma((2, 2)), dma((4 * NCH,)), dma((4 * NCH,)),
-            dma((2, 2)), dma((4,)), dma((len(TABLE),)), dma((len(TABLE),)),
+            dma((4,)), dma((2, 3)), dma((2, 4)), dma((2, 2)), dma((4 * NCH,)), dma((4 * NCH,)),
+            dma((2, 2)), dma((4,)), dma((len(TABLE),)), dma((len(TABLE),)), dma((2 * len(LANES),)),
         ],
         compiler_params=pltpu.CompilerParams(
             collective_id=0, has_side_effects=True, vmem_limit_bytes=60 * 2**20),
     )(inputs, cotangent, w_up, w_down)
-    grad_up, grad_down = pl.pallas_call(
+    return pl.pallas_call(
         widen,
         name="widen",
-        grid=(8,),
-        out_shape=(jax.ShapeDtypeStruct((HALF, HID), F32), jax.ShapeDtypeStruct((HID, HALF), F32)),
-        in_specs=[pl.BlockSpec((4096, 128), lambda i: (i, 0))],
-        out_specs=(
-            pl.BlockSpec((HALF, 512), lambda i: (0, i // 4 * 2 + jnp.minimum(lax.rem(i, 4), 1))),
-            pl.BlockSpec((HALF, 512), lambda i: (i // 4, jnp.maximum(lax.rem(i, 4) - 2, 0)))),
-    )(sums)
-    return grad_inputs, grad_up, grad_down
+        out_shape=(gin_shape, jax.ShapeDtypeStruct((HALF, HID), F32), jax.ShapeDtypeStruct((HID, HALF), F32)),
+        in_specs=[anywhere] * 2,
+        out_specs=(anywhere,) * 3,
+        scratch_shapes=[
+            pltpu.VMEM((TOK, HALF), BF16), pltpu.VMEM((2 * ROWS, 128), BF16),
+            pltpu.VMEM((HALF, 2 * HID), F32),
+            dma((2,)), dma((PARTS,)), dma((PARTS,)),
+        ],
+        compiler_params=pltpu.CompilerParams(vmem_limit_bytes=60 * 2**20),
+    )(grad_inputs, sums)
 
 
 def solution(mesh):

time: 147 us -> 132 us (0.90)
  Pallas kernels: 145 us -> 131 us
    pallas_call x2, Pallas kernels: 145 us -> 131 us  [the longest x1 122 us: shards(): pl.pallas_call(body, name='ffn_backward', out_shape=(gin_shape, jax.Shape...]
where the time goes in v3:
time: 132 us
  Pallas kernels  131 us (99%)
    pallas_call x1, Pallas kernels, shards(): pl.pallas_call(body, name='ffn_backward', out_shape=(gin_shape, jax.Shape...  122 us
    pallas_call x1, Pallas kernels, shards(): pl.pallas_call(widen, name='widen', out_shape=(gin_shape, jax.ShapeDtypeS...  9.54 us

profile of v3, /device:TPU:8, one launch (start us, length us, event | category | flops | bytes accessed | tf_op | source)
XLA Modules:
  0.0 132.0 jit_solution(8539973716402905167)
XLA Ops:
  0.6 121.7 %ffn_backward.1 = (bf16[128,1024]{1,0:T(8,128)(2,1)}, bf16[32768,128]{1,0:T(8,128)(2,1)}) custom-call(bf16[128,1024]{1,0:T(8,128)(2,1)} %in_ref.1, bf16[128,1024]{1,0:T(8,128)(2,1)} %cot_ref.1, bf16[1024,2048]{1,0:T(8,128)(2,1)} %up_ref.1, bf16[2048,1024]{1,0:T(8,128)(2,1)} %down_ref.1), custom_call_target="tpu_custom_call" | custom-call | tf_op jit(solution)/shard_map/ffn_backward/pallas_call | solution.py:497
  122.3 9.5 %widen.1 = (bf16[128,1024]{1,0:T(8,128)(2,1)}, f32[1024,2048]{1,0:T(8,128)}, f32[2048,1024]{1,0:T(8,128)}) custom-call(bf16[128,1024]{1,0:T(8,128)(2,1)} %get-tuple-element.5.gin_ref, bf16[32768,128]{1,0:T(8,128)(2,1)} %get-tuple-element.6.sums_ref), custom_call_target="tpu_custom_call" | custom-call | tf_op jit(solution)/shard_map/widen/pallas_call | solution.py:520

commit v4 on v3

--- a/solution.py
+++ b/solution.py
@@ -20,21 +20,29 @@
 ROWS = 2 * HALF * QUARTER // 128
 TILE = 16
 A, B = ("y", "z"), ("z", "y")
-LANES = ((*A, 1, 3), (*B, -1, 2), (*A, -1, 3), (*B, 1, 2), (*A, 1, 3), (*B, -1, 2), (*A, -1, 3),
-         (*A, 1, 3), (*B, 1, 2), (*A, -1, 3), (*B, -1, 2), (*A, 1, 1), (*B, 1, 2), (*A, -1, 1))
+LANES = (
+    (*A, 1, 2, True), (*B, -1, 2, True), (*A, -1, 3, True), (*B, 1, 2, True),
+    (*A, 1, 3, True), (*B, -1, 2, False), (*A, -1, 3, False), (*A, 1, 3, False),
+    (*B, 1, 2, False), (*A, -1, 2, False), (*B, 1, 2, False), (*A, 1, 2, False),
+    (*B, 1, 2, False), (*B, -1, 2, False),
+)
 UPTO = tuple(sum(lane[3] for lane in LANES[:i + 1]) for i in range(len(LANES)))
 STARTS = tuple(2.4 * tiles / 32 for tiles in UPTO)
 PIECES = NY * NZ
 RATE, LAG, WINDOW, WORK = 46000.0, 2.0, 1.6, 0.12
+XFREE = 20.0
 RANKS = {
-    "rs1": (8, 39, 32, 19, 44, 56, 71, 34, 12, 58, 65, 47, 29, 68),
-    "rs2": (16, 70, 64, 91, 37, 17, 83, 21, 78, 72, 95, 84, 80, 87),
-    "x": (46, 59, 52, 74, 51, 3, 48, 0, 61, 50, 18, 88, 41, 9),
-    "ag2": (35, 24, 40, 62, 13, 94, 77, 55, 57, 67, 85, 66, 27, 43),
-    "ag1": (42, 97, 75, 38, 10, 14, 11, 2, 81, 86, 54, 53, 79, 45),
-    "far2": (4, 33, 22, 23, 31, 30, 73, 63, 82, 5, 49, 69, 28, 60),
-    "far1": (15, 89, 1, 76, 25, 90, 92, 7, 96, 26, 6, 36, 20, 93)}
-FIRST = ("rs1", "ag1", "far1")
+    "rs1": (44, 18, 24, 107, 45, 37, 92, 14, 50, 77, 111, 62, 95, 110),
+    "rs2": (27, 85, 11, 79, 84, 8, 80, 97, 83, 55, 87, 10, 93, 31),
+    "x": (54, 75, 96, 39, 91, 104, 35, 63, 29, 34, 76, 82, 17, 43),
+    "ag2": (49, 81, 9, 109, 12, 25, 66, 52, 51, 60, 101, 58, 53, 42),
+    "ag1": (7, 67, 22, 90, 15, 86, 89, 40, 105, 108, 98, 57, 99, 74),
+    "far2": (59, 78, 70, 65, 88, 69, 26, 6, 3, 19, 33, 0, 64, 1),
+    "far1": (41, 56, 30, 48, 72, 100, 20, 13, 4, 68, 16, 71, 102, 2),
+    "xl": (103, 36, 5, 47, 38, 46, 23, 32, 73, 61, 94, 21, 106, 28),
+}
+FIRST = ("rs1", "ag1", "far1", "xl")
+SENDING = 24
 
 
 def hops(n, arm):
@@ -54,19 +62,31 @@
     return phase == "x" or k == hops(RINGS[ring_of(lane, phase)], arm)
 
 
+def way_of(lane, phase, arm):
+    if phase in ("x", "xl"):
+        return "x", 0
+    way = LANES[lane][2] if arm == 0 else -LANES[lane][2]
+    return ring_of(lane, phase), -way if phase[:2] == "rs" else way
+
+
+def arrivals(lane, phase):
+    n = RINGS[ring_of(lane, phase)]
+    if phase == "x":
+        return [(lane, phase, 0, 1)]
+    if phase == "xl":
+        return [(lane, phase, 0, 0)] + [(lane, phase, arm, k) for arm in (0, 1) for k in range(1, hops(n, arm) + 1)]
+    if phase == "ag1" and LANES[lane][4]:
+        return []
+    return [(lane, phase, arm, hops(n, arm)) for arm in (0, 1)]
+
+
 def planned():
-    order, free, ready, flying, joined, now, count = [], {}, {}, [], {}, 0.0, 0
-
-    def link_of(lane, phase, arm):
-        if phase == "x":
-            return "x"
-        way = LANES[lane][2] if arm == 0 else -LANES[lane][2]
-        return ring_of(lane, phase), -way if phase[:2] == "rs" else way
+    order, free, ready, flying, joined, now, count = [], {"x": XFREE}, {}, [], {}, 0.0, 0
 
     def want(lane, phase, arm, k):
         nonlocal count
         count += 1
-        line = ready.setdefault(link_of(lane, phase, arm), [])
+        line = ready.setdefault(way_of(lane, phase, arm), [])
         heapq.heappush(line, (RANKS[phase][lane], -k, count, (lane, phase, arm, k)))
 
     def begin(lane, phase):
@@ -74,15 +94,18 @@
         for arm in (0,) if phase == "x" else (0, 1):
             want(lane, phase, arm, 1)
 
+    def clear(link):
+        return free.get("x" if link[0] == "x" else link, 0.0)
+
     def issue():
         nonlocal count
         for link, line in ready.items():
-            while line and max(now, free.get(link, 0.0)) - now < WINDOW:
+            while line and max(now, clear(link)) - now < WINDOW:
                 what = heapq.heappop(line)[3]
-                cost = length(what[0], what[1]) * 256 * (2 if link == "x" else 1) / RATE
-                free[link] = max(now, free.get(link, 0.0)) + cost
+                done = max(now, clear(link)) + length(what[0], what[1]) * 256 / RATE
+                free["x" if link[0] == "x" else link] = done
                 count += 1
-                heapq.heappush(flying, (free[link] + LAG, count, what))
+                heapq.heappush(flying, (done + LAG, count, what))
                 order.append(("send",) + what)
 
     todo = sorted((at, lane) for lane, at in enumerate(STARTS))
@@ -94,20 +117,41 @@
             begin(lane, "rs1")
         else:
             at, _, (lane, phase, arm, k) = heapq.heappop(flying)
-            now = max(now, at) + WORK
-            if not last(lane, phase, arm, k):
+            now = max(now, at)
+            late = LANES[lane][4]
+            if phase == "xl":
+                joined[lane, phase] += 1
+                if joined[lane, phase] == RINGS[LANES[lane][0]]:
+                    order.append(("end", lane, phase))
+                    now += WORK
+            elif late and phase == "ag1":
+                now += WORK
+                order.append(("pass", lane, phase, arm, k))
+                if not last(lane, phase, arm, k):
+                    want(lane, phase, arm, k + 1)
+                else:
+                    joined[lane, phase] += 1
+                    if joined[lane, phase] == 2:
+                        order.append(("end", lane, phase))
+                want(lane, "xl", arm, k)
+            elif not last(lane, phase, arm, k):
+                now += WORK
                 order.append(("pass", lane, phase, arm, k))
                 want(lane, phase, arm, k + 1)
             else:
                 joined[lane, phase] += 1
                 if phase == "x" or joined[lane, phase] == 2:
+                    now += WORK
                     order.append(("end", lane, phase))
-                    for after in {"rs1": ("rs2",), "rs2": ("x", "ag2"), "x": ("far2",),
+                    for after in {"rs1": ("rs2",), "rs2": ("ag2",) if late else ("x", "ag2"), "x": ("far2",),
                                   "ag2": ("ag1",), "far2": ("far1",)}.get(phase, ()):
                         begin(lane, after)
+                    if late and phase == "ag2":
+                        joined[lane, "xl"] = 0
+                        want(lane, "xl", 0, 0)
         issue()
         if not flying and not todo and any(ready.values()):
-            now = min(free[link] for link, line in ready.items() if line)
+            now = min(clear(link) for link, line in ready.items() if line)
             issue()
     return order, now
 
@@ -116,18 +160,36 @@
 
 
 def transfers():
-    table, rows = {}, 0
-    for lane in range(len(LANES)):
-        for phase in ("rs1", "rs2", "x", "ag2", "ag1", "far2", "far1"):
-            for arm in (0,) if phase == "x" else (0, 1):
-                for k in range(1, 2 if phase == "x" else hops(RINGS[ring_of(lane, phase)], arm) + 1):
-                    lands = phase[:2] == "rs"
-                    table[lane, phase, arm, k] = (len(table), rows if lands else None)
-                    rows += length(lane, phase) if lands else 0
-    return table, rows
-
-
-TABLE, LANDING = transfers()
+    sent, waited = {}, {}
+    for at, step in enumerate(ORDER):
+        if step[0] == "send":
+            sent[step[1:]] = at
+        elif step[0] == "pass":
+            waited[step[1:]] = at
+        elif step[0] == "end":
+            waited.update((what, at) for what in arrivals(*step[1:]))
+    table, rows, slots, back = {}, 0, [], {}
+    for what in sent:
+        back.setdefault(way_of(*what[:3]), []).append((sent[what], waited[what]))
+    for what in sorted(sent, key=sent.get):
+        ring, way = way_of(*what[:3])
+        chosen = None
+        for i, (link, free) in enumerate(slots):
+            if link == (ring, way) and free < sent[what]:
+                chosen = i
+                break
+        if chosen is None:
+            chosen = len(slots)
+            slots.append(None)
+        heard = [end for begin, end in back[ring, -way] if begin > waited[what]]
+        slots[chosen] = (ring, way), min(heard, default=len(ORDER))
+        lands = what[1][:2] == "rs"
+        table[what] = (chosen, rows if lands else None)
+        rows += length(what[0], what[1]) if lands else 0
+    return table, rows, len(slots)
+
+
+TABLE, LANDING, RECEIVING = transfers()
 
 
 def dot(a, b, dims):
@@ -342,7 +404,7 @@
     for lane in range(len(LANES)):
         bases.append(base)
         base += LANES[lane][3] * TILE * PIECES
-    started = {}
+    started, outgoing = {}, []
 
     def chunk(lane, phase, step):
         ring = ring_of(lane, phase)
@@ -350,7 +412,7 @@
         start = bases[lane]
         if phase not in FIRST:
             start += pos[LANES[lane][0]] * length(lane, "rs1")
-        if phase[:2] == "ag" or phase == "x":
+        if phase[:2] == "ag" or phase in ("x", "xl"):
             start += xh * ROWS
         elif phase[:3] == "far":
             start += (1 - xh) * ROWS
@@ -364,6 +426,10 @@
         way = LANES[lane][2] if arm == 0 else -LANES[lane][2]
         if phase == "x":
             begin, rows = chunk(lane, phase, 0)
+            src = dst = out_ref.at[pl.ds(begin, rows)]
+            who = xpeer
+        elif phase == "xl":
+            begin, rows = chunk(lane, phase, -k if arm == 0 else k)
             src = dst = out_ref.at[pl.ds(begin, rows)]
             who = xpeer
         elif slot is not None:
@@ -374,8 +440,11 @@
             begin, rows = chunk(lane, phase, 1 - k if arm == 0 else k - 1)
             src = dst = out_ref.at[pl.ds(begin, rows)]
             who = at(ring, way)
-        copy = remote(src, dst, ss.at[index], rs.at[index], who)
+        if len(outgoing) >= SENDING:
+            outgoing[-SENDING].wait_send()
+        copy = remote(src, dst, ss.at[len(outgoing) % SENDING], rs.at[index], who)
         copy.start()
+        outgoing.append(copy)
         started[lane, phase, arm, k] = copy
 
     def add(target, shift, begin, slots, rows):
@@ -412,20 +481,20 @@
                 aside.pop(0)()
         else:
             phase = step[2]
-            n = RINGS[ring_of(lane, phase)]
-            ends = [(lane, phase, 0, 1)] if phase == "x" else [
-                (lane, phase, arm, hops(n, arm)) for arm in (0, 1)]
+            ends = arrivals(lane, phase)
             for which in ends:
                 started[which].wait_recv()
             if phase[:2] == "rs":
                 begin, rows = chunk(lane, phase, 0)
                 into, shift = (g, 0) if phase == "rs1" else (out_ref, xh * ROWS)
                 add(into, shift, begin, [TABLE[which][1] for which in ends], rows)
-            elif phase in ("ag1", "far1"):
+            elif phase in ("ag1", "far1", "xl"):
                 half = xh if phase == "ag1" else 1 - xh
                 there = pl.ds(pl.multiple_of(half * ROWS + bases[lane], TILE), LANES[lane][3] * TILE * PIECES)
+                if len(leaving) >= 4:
+                    leaving[-4].wait()
                 leaving.append(pltpu.make_async_copy(
-                    out_ref.at[there], sums_ref.at[there], os.at[len(leaving)]))
+                    out_ref.at[there], sums_ref.at[there], os.at[len(leaving) % 4]))
                 leaving[-1].start()
         if count == len(ORDER) * 3 // 5:
             inputs_sum()
@@ -450,9 +519,9 @@
     @pl.when(away)
     def _():
         give(0, f).wait_send()
-    for copy in started.values():
+    for copy in outgoing[-SENDING:]:
         copy.wait_send()
-    for copy in leaving:
+    for copy in leaving[-4:]:
         copy.wait()
 
 
@@ -512,7 +581,7 @@
             pltpu.VMEM((ROWS, 128), BF16), pltpu.VMEM((LANDING, 128), BF16),
             pltpu.VMEM((2 * GRP, HALF), BF16), pltpu.VMEM((4, TOK, HALF), BF16),
             dma((4,)), dma((2, 3)), dma((2, 4)), dma((2, 2)), dma((4 * NCH,)), dma((4 * NCH,)),
-            dma((2, 2)), dma((4,)), dma((len(TABLE),)), dma((len(TABLE),)), dma((2 * len(LANES),)),
+            dma((2, 2)), dma((4,)), dma((SENDING,)), dma((RECEIVING,)), dma((4,)),
         ],
         compiler_params=pltpu.CompilerParams(
             collective_id=0, has_side_effects=True, vmem_limit_bytes=60 * 2**20),

time: 132 us -> 117 us (0.89)
  Pallas kernels: 131 us -> 116 us
    pallas_call x1, Pallas kernels: 122 us -> 106 us  [shards(): pl.pallas_call(body, name='ffn_backward', out_shape=(gin_shape, jax.Shape...]
where the time goes in v4:
time: 117 us
  Pallas kernels  116 us (99%)
    pallas_call x1, Pallas kernels, shards(): pl.pallas_call(body, name='ffn_backward', out_shape=(gin_shape, jax.Shape...  106 us
    pallas_call x1, Pallas kernels, shards(): pl.pallas_call(widen, name='widen', out_shape=(gin_shape, jax.ShapeDtypeS...  9.54 us

profile of v4, /device:TPU:8, one launch (start us, length us, event | category | flops | bytes accessed | tf_op | source)
XLA Modules:
  0.0 116.8 jit_solution(10571040198511144088)
XLA Ops:
  0.6 106.5 %ffn_backward.1 = (bf16[128,1024]{1,0:T(8,128)(2,1)}, bf16[32768,128]{1,0:T(8,128)(2,1)}) custom-call(bf16[128,1024]{1,0:T(8,128)(2,1)} %in_ref.1, bf16[128,1024]{1,0:T(8,128)(2,1)} %cot_ref.1, bf16[1024,2048]{1,0:T(8,128)(2,1)} %up_ref.1, bf16[2048,1024]{1,0:T(8,128)(2,1)} %down_ref.1), custom_call_target="tpu_custom_call" | custom-call | tf_op jit(solution)/shard_map/ffn_backward/pallas_call | solution.py:566
  107.1 9.5 %widen.1 = (bf16[128,1024]{1,0:T(8,128)(2,1)}, f32[1024,2048]{1,0:T(8,128)}, f32[2048,1024]{1,0:T(8,128)}) custom-call(bf16[128,1024]{1,0:T(8,128)(2,1)} %get-tuple-element.5.gin_ref, bf16[32768,128]{1,0:T(8,128)(2,1)} %get-tuple-element.6.sums_ref), custom_call_target="tpu_custom_call" | custom-call | tf_op jit(solution)/shard_map/widen/pallas_call | solution.py:589

commit v5 on v4

--- a/solution.py
+++ b/solution.py
@@ -21,25 +21,25 @@
 TILE = 16
 A, B = ("y", "z"), ("z", "y")
 LANES = (
-    (*A, 1, 2, True), (*B, -1, 2, True), (*A, -1, 3, True), (*B, 1, 2, True),
-    (*A, 1, 3, True), (*B, -1, 2, False), (*A, -1, 3, False), (*A, 1, 3, False),
-    (*B, 1, 2, False), (*A, -1, 2, False), (*B, 1, 2, False), (*A, 1, 2, False),
-    (*B, 1, 2, False), (*B, -1, 2, False),
+    (*B, -1, 2, True), (*B, 1, 2, True), (*A, -1, 2, False), (*B, -1, 2, False),
+    (*A, 1, 2, True), (*A, 1, 2, False), (*B, 1, 2, False), (*B, 1, 2, False),
+    (*B, -1, 2, False), (*A, 1, 2, False), (*B, 1, 2, False), (*A, 1, 2, True),
+    (*A, -1, 2, False), (*A, -1, 2, False), (*A, 1, 2, True), (*A, -1, 2, True),
 )
 UPTO = tuple(sum(lane[3] for lane in LANES[:i + 1]) for i in range(len(LANES)))
 STARTS = tuple(2.4 * tiles / 32 for tiles in UPTO)
 PIECES = NY * NZ
-RATE, LAG, WINDOW, WORK = 46000.0, 2.0, 1.6, 0.12
+RATE, LAG, WINDOW, WORK = 46000.0, 2.0, 1.2, 0.12
 XFREE = 20.0
 RANKS = {
-    "rs1": (44, 18, 24, 107, 45, 37, 92, 14, 50, 77, 111, 62, 95, 110),
-    "rs2": (27, 85, 11, 79, 84, 8, 80, 97, 83, 55, 87, 10, 93, 31),
-    "x": (54, 75, 96, 39, 91, 104, 35, 63, 29, 34, 76, 82, 17, 43),
-    "ag2": (49, 81, 9, 109, 12, 25, 66, 52, 51, 60, 101, 58, 53, 42),
-    "ag1": (7, 67, 22, 90, 15, 86, 89, 40, 105, 108, 98, 57, 99, 74),
-    "far2": (59, 78, 70, 65, 88, 69, 26, 6, 3, 19, 33, 0, 64, 1),
-    "far1": (41, 56, 30, 48, 72, 100, 20, 13, 4, 68, 16, 71, 102, 2),
-    "xl": (103, 36, 5, 47, 38, 46, 23, 32, 73, 61, 94, 21, 106, 28),
+    "rs1": (15, 121, 3, 111, 7, 93, 115, 43, 98, 65, 127, 92, 23, 49, 55, 12),
+    "rs2": (71, 8, 37, 95, 125, 78, 85, 126, 0, 76, 17, 107, 84, 68, 32, 29),
+    "x": (91, 73, 57, 74, 39, 24, 105, 103, 34, 81, 62, 59, 83, 75, 53, 42),
+    "ag2": (99, 72, 101, 94, 88, 64, 100, 56, 30, 20, 120, 67, 16, 11, 33, 45),
+    "ag1": (19, 96, 90, 119, 1, 52, 28, 108, 87, 38, 110, 35, 89, 9, 50, 10),
+    "far2": (4, 69, 82, 77, 80, 46, 66, 70, 116, 60, 31, 5, 2, 14, 51, 102),
+    "far1": (40, 124, 97, 113, 117, 41, 109, 27, 112, 122, 79, 47, 118, 21, 44, 54),
+    "xl": (114, 106, 86, 25, 18, 61, 26, 104, 63, 6, 22, 123, 36, 13, 58, 48),
 }
 FIRST = ("rs1", "ag1", "far1", "xl")
 SENDING = 24
@@ -56,6 +56,10 @@
 def length(lane, phase):
     piece = LANES[lane][3] * TILE
     return piece * RINGS[LANES[lane][1]] if phase in FIRST else piece
+
+
+def lane_rows(lane):
+    return LANES[lane][3] * TILE * PIECES
 
 
 def last(lane, phase, arm, k):
@@ -196,9 +200,10 @@
     return lax.dot_general(a, b, (dims, ((), ())), preferred_element_type=F32)
 
 
-def body(in_ref, cot_ref, up_ref, down_ref, gin_ref, sums_ref,
-         in_v, cot_v, out_ref, x, c, xt, sqt, up, down, p_own, p_far, a_own, a_out, a_far, pre, sq, g, land, r, r_in,
-         local_sem, xs, xr, fsem, ds, dr, gs, gr, ss, rs, os):
+def body(in_ref, cot_ref, up_ref, down_ref, gin_ref, *refs):
+    outs = refs[:len(LANES)]
+    (in_v, cot_v, x, c, xt, sqt, up, down, p_own, p_far, a_own, a_out, a_far, pre, sq, g, land, r, r_in,
+     local_sem, xs, xr, fsem, ds, dr, gs, gr, ss, rs) = refs[len(LANES):]
     rep, f, t = lax.axis_index("rep"), lax.axis_index("fs"), lax.axis_index("tp")
     xh = lax.rem(rep, NX)
     yz = rep // NX
@@ -409,13 +414,14 @@
     def chunk(lane, phase, step):
         ring = ring_of(lane, phase)
         rows = length(lane, phase)
-        start = bases[lane]
+        if phase[:2] == "rs":
+            start = bases[lane]
+        elif phase[:3] == "far":
+            start = (1 - xh) * lane_rows(lane)
+        else:
+            start = xh * lane_rows(lane)
         if phase not in FIRST:
             start += pos[LANES[lane][0]] * length(lane, "rs1")
-        if phase[:2] == "ag" or phase in ("x", "xl"):
-            start += xh * ROWS
-        elif phase[:3] == "far":
-            start += (1 - xh) * ROWS
         n = RINGS[ring]
         there = lax.rem(pos[ring] + LANES[lane][2] * step + n, n)
         return pl.multiple_of(start + there * rows, TILE), rows
@@ -426,11 +432,11 @@
         way = LANES[lane][2] if arm == 0 else -LANES[lane][2]
         if phase == "x":
             begin, rows = chunk(lane, phase, 0)
-            src = dst = out_ref.at[pl.ds(begin, rows)]
+            src = dst = outs[lane].at[pl.ds(begin, rows)]
             who = xpeer
         elif phase == "xl":
             begin, rows = chunk(lane, phase, -k if arm == 0 else k)
-            src = dst = out_ref.at[pl.ds(begin, rows)]
+            src = dst = outs[lane].at[pl.ds(begin, rows)]
             who = xpeer
         elif slot is not None:
             left = hops(RINGS[ring], arm) - k + 1
@@ -438,7 +444,7 @@
             src, dst, who = g.at[pl.ds(begin, rows)], land.at[pl.ds(slot, rows)], at(ring, -way)
         else:
             begin, rows = chunk(lane, phase, 1 - k if arm == 0 else k - 1)
-            src = dst = out_ref.at[pl.ds(begin, rows)]
+            src = dst = outs[lane].at[pl.ds(begin, rows)]
             who = at(ring, way)
         if len(outgoing) >= SENDING:
             outgoing[-SENDING].wait_send()
@@ -459,7 +465,6 @@
             target[pl.ds(pl.multiple_of(here + shift, TILE), unit), :] = total.astype(BF16)
 
     aside = [functools.partial(inputs_part, j) for j in range(4)] + [give_all]
-    leaving = []
     begun = chunks = 0
     for count, step in enumerate(ORDER):
         kind, lane = step[:2]
@@ -486,16 +491,8 @@
                 started[which].wait_recv()
             if phase[:2] == "rs":
                 begin, rows = chunk(lane, phase, 0)
-                into, shift = (g, 0) if phase == "rs1" else (out_ref, xh * ROWS)
+                into, shift = (g, 0) if phase == "rs1" else (outs[lane], xh * lane_rows(lane) - bases[lane])
                 add(into, shift, begin, [TABLE[which][1] for which in ends], rows)
-            elif phase in ("ag1", "far1", "xl"):
-                half = xh if phase == "ag1" else 1 - xh
-                there = pl.ds(pl.multiple_of(half * ROWS + bases[lane], TILE), LANES[lane][3] * TILE * PIECES)
-                if len(leaving) >= 4:
-                    leaving[-4].wait()
-                leaving.append(pltpu.make_async_copy(
-                    out_ref.at[there], sums_ref.at[there], os.at[len(leaving) % 4]))
-                leaving[-1].start()
         if count == len(ORDER) * 3 // 5:
             inputs_sum()
 
@@ -521,40 +518,43 @@
         give(0, f).wait_send()
     for copy in outgoing[-SENDING:]:
         copy.wait_send()
-    for copy in leaving[-4:]:
-        copy.wait()
 
 
 PARTS = 8
 
 
-def widen(gin_ref, sums_ref, gin_out, up_out, down_out, gin, narrow, wide, sem, read, write):
-    through = pltpu.make_async_copy(gin_ref, gin, sem.at[0])
+def pieces(column):
+    found, first, end = [], column * HALF, (column + 1) * HALF
+    for lane in range(len(LANES)):
+        low = (UPTO[lane] - LANES[lane][3]) * TILE * PIECES
+        begin, stop = max(first, low), min(end, low + lane_rows(lane))
+        if begin < stop:
+            found.append((lane, begin - low, begin - first, stop - begin))
+    return found
+
+
+def widen(gin_ref, *refs):
+    sums = refs[:len(LANES)]
+    gin_out, up_out, down_out, wide, sem, write = refs[len(LANES):]
+    through = pltpu.make_async_copy(gin_ref, gin_out, sem)
     through.start()
-    rows, columns = 2 * ROWS // PARTS, 2 * ROWS // PARTS // HALF
-    reads = []
-    for i in range(PARTS):
-        there = pl.ds(i * rows, rows)
-        reads.append(pltpu.make_async_copy(sums_ref.at[there], narrow.at[there], read.at[i]))
-        reads[i].start()
+    columns = 2 * ROWS // PARTS // HALF
     writes = []
     for i in range(PARTS):
-        reads[i].wait()
         first = i * columns
-        for j in range(first, first + columns):
-            wide[:, j * 128:(j + 1) * 128] = narrow[j * HALF:(j + 1) * HALF, :].astype(F32)
         half, column = first // 16, first % 16
+        for j in range(columns):
+            for lane, row, there, rows in pieces(column + j):
+                row += half * lane_rows(lane)
+                wide[there:there + rows, (first + j) * 128:(first + j + 1) * 128] = (
+                    sums[lane][row:row + rows, :].astype(F32))
         if column < 8:
             there = up_out.at[:, pl.ds(half * QUARTER + column * 128, columns * 128)]
         else:
             there = down_out.at[pl.ds(half * QUARTER, QUARTER), pl.ds((column - 8) * 128, columns * 128)]
         writes.append(pltpu.make_async_copy(wide.at[:, pl.ds(first * 128, columns * 128)], there, write.at[i]))
         writes[i].start()
-        if i == 0:
-            through.wait()
-            back = pltpu.make_async_copy(gin, gin_out, sem.at[1])
-            back.start()
-    back.wait()
+    through.wait()
     for copy in writes:
         copy.wait()
 
@@ -563,14 +563,14 @@
     vmem, anywhere = pl.BlockSpec(memory_space=pltpu.VMEM), pl.BlockSpec(memory_space=pl.ANY)
     gin_shape = jax.ShapeDtypeStruct((TOK, HALF), BF16)
     dma = pltpu.SemaphoreType.DMA
-    grad_inputs, sums = pl.pallas_call(
+    grad_inputs, *sums = pl.pallas_call(
         body,
         name="ffn_backward",
-        out_shape=(gin_shape, jax.ShapeDtypeStruct((2 * ROWS, 128), BF16)),
+        out_shape=(gin_shape, *(jax.ShapeDtypeStruct((2 * lane_rows(lane), 128), BF16) for lane in range(len(LANES)))),
         in_specs=[anywhere] * 4,
-        out_specs=(vmem, anywhere),
+        out_specs=(vmem,) * (1 + len(LANES)),
         scratch_shapes=[
-            pltpu.VMEM((TOK, HALF), BF16), pltpu.VMEM((TOK, HALF), BF16), pltpu.VMEM((2 * ROWS, 128), BF16),
+            pltpu.VMEM((TOK, HALF), BF16), pltpu.VMEM((TOK, HALF), BF16),
             pltpu.VMEM((2 * GRP, HALF), BF16), pltpu.VMEM((2 * GRP, HALF), BF16),
             pltpu.VMEM((HALF, 2 * GRP), BF16), pltpu.VMEM((QUARTER, 2 * GRP), BF16),
             pltpu.VMEM((HALF, QUARTER), BF16), pltpu.VMEM((QUARTER, HALF), BF16),
@@ -581,24 +581,22 @@
             pltpu.VMEM((ROWS, 128), BF16), pltpu.VMEM((LANDING, 128), BF16),
             pltpu.VMEM((2 * GRP, HALF), BF16), pltpu.VMEM((4, TOK, HALF), BF16),
             dma((4,)), dma((2, 3)), dma((2, 4)), dma((2, 2)), dma((4 * NCH,)), dma((4 * NCH,)),
-            dma((2, 2)), dma((4,)), dma((SENDING,)), dma((RECEIVING,)), dma((4,)),
+            dma((2, 2)), dma((4,)), dma((SENDING,)), dma((RECEIVING,)),
         ],
         compiler_params=pltpu.CompilerParams(
-            collective_id=0, has_side_effects=True, vmem_limit_bytes=60 * 2**20),
+            collective_id=0, has_side_effects=True, vmem_limit_bytes=45 * 2**20),
     )(inputs, cotangent, w_up, w_down)
     return pl.pallas_call(
         widen,
         name="widen",
         out_shape=(gin_shape, jax.ShapeDtypeStruct((HALF, HID), F32), jax.ShapeDtypeStruct((HID, HALF), F32)),
-        in_specs=[anywhere] * 2,
+        in_specs=[vmem] * (1 + len(LANES)),
         out_specs=(anywhere,) * 3,
         scratch_shapes=[
-            pltpu.VMEM((TOK, HALF), BF16), pltpu.VMEM((2 * ROWS, 128), BF16),
-            pltpu.VMEM((HALF, 2 * HID), F32),
-            dma((2,)), dma((PARTS,)), dma((PARTS,)),
+            pltpu.VMEM((HALF, 2 * HID), F32), dma, dma((PARTS,)),
         ],
-        compiler_params=pltpu.CompilerParams(vmem_limit_bytes=60 * 2**20),
-    )(grad_inputs, sums)
+        compiler_params=pltpu.CompilerParams(vmem_limit_bytes=26 * 2**20),
+    )(grad_inputs, *sums)
 
 
 def solution(mesh):

time: 117 us -> 113 us (0.966)
  Pallas kernels: 116 us -> 110 us
  local copies, waits for them, and re-layouts: 0 us -> 1.89 us
    pallas_call x1, Pallas kernels: 9.54 us -> 6.3 us  [shards(): pl.pallas_call(widen, name='widen', out_shape=(gin_shape, jax.ShapeDtypeS...]
    pallas_call x1, Pallas kernels: 106 us -> 104 us  [shards(): pl.pallas_call(body, name='ffn_backward', out_shape=(gin_shape, *(jax.Sha...]
    unnamed x0 -> x4, local copies, waits for them, and re-layouts: none -> 1.89 us
where the time goes in v5:
time: 113 us
  Pallas kernels  110 us (97%)
  local copies, waits for them, and re-layouts  1.89 us (2%)
    pallas_call x1, Pallas kernels, shards(): pl.pallas_call(body, name='ffn_backward', out_shape=(gin_shape, *(jax.Sha...  104 us
    pallas_call x1, Pallas kernels, shards(): pl.pallas_call(widen, name='widen', out_shape=(gin_shape, jax.ShapeDtypeS...  6.3 us

profile of v5, /device:TPU:8, one launch (start us, length us, event | category | flops | bytes accessed | tf_op | source)
XLA Modules:
  0.0 112.9 jit_solution(15936524731367038336)
XLA Ops:
  0.6 0.0 copy-start
  0.6 0.9 copy-done
  1.6 0.0 copy-start.1
  1.6 0.9 copy-done.1
  2.5 103.9 %ffn_backward.1 = (bf16[128,1024]{1,0:T(8,128)(2,1)S(1)}, bf16[2048,128]{1,0:T(8,128)(2,1)S(1)}, bf16[2048,128]{1,0:T(8,128)(2,1)S(1)}, bf16[2048,128]{1,0:T(8,1...) custom-call(bf16[128,1024]{1,0:T(8,128)(2,1)S(1)} %copy-done, ...), custom_call_target="tpu_custom_call" | custom-call | tf_op jit(solution)/shard_map/ffn_backward/pallas_call | solution.py:566
  106.4 6.3 %widen.1 = (bf16[128,1024]{1,0:T(8,128)(2,1)}, f32[1024,2048]{1,0:T(8,128)}, f32[2048,1024]{1,0:T(8,128)}) custom-call(bf16[128,1024]{1,0:T(8,128)(2,1)S(1)} %get-tuple-element.20.gin_ref, bf16[2048,128]{1,0:T(8,128)(2,1)S(1)} %get-tuple-element.21.refs_0_, bf16[2048,128]{1,0:T(8,128)(2,1)S(1)} %get-tuple-element.22.refs_1_, ...), custom_call_target="tpu_custom_call" | custom-call | tf_op jit(solution)/shard_map/widen/pallas_call | solution.py:589
Async XLA Ops:
  0.6 1.0 copy-start
  1.6 0.9 copy-start.1

commit v6 on v5

--- a/solution.py
+++ b/solution.py
@@ -585,7 +585,7 @@
         ],
         compiler_params=pltpu.CompilerParams(
             collective_id=0, has_side_effects=True, vmem_limit_bytes=45 * 2**20),
-    )(inputs, cotangent, w_up, w_down)
+    )(pltpu.with_memory_space_constraint(inputs, pltpu.HBM), pltpu.with_memory_space_constraint(cotangent, pltpu.HBM), w_up, w_down)
     return pl.pallas_call(
         widen,
         name="widen",

time: 113 us -> 111 us (0.982)
  local copies, waits for them, and re-layouts: 1.89 us -> 0 us
    unnamed x4 -> x0, local copies, waits for them, and re-layouts: 1.89 us -> none
where the time goes in v6:
time: 111 us
  Pallas kernels  110 us (99%)
    pallas_call x1, Pallas kernels, shards(): pl.pallas_call(body, name='ffn_backward', out_shape=(gin_shape, *(jax.Sha...  104 us
    pallas_call x1, Pallas kernels, shards(): pl.pallas_call(widen, name='widen', out_shape=(gin_shape, jax.ShapeDtypeS...  6.3 us

profile of v6, /device:TPU:8, one launch (start us, length us, event | category | flops | bytes accessed | tf_op | source)
XLA Modules:
  0.0 111.2 jit_solution(3432192490675307883)
XLA Ops:
  0.6 104.1 %ffn_backward.1 = (bf16[128,1024]{1,0:T(8,128)(2,1)S(1)}, bf16[2048,128]{1,0:T(8,128)(2,1)S(1)}, bf16[2048,128]{1,0:T(8,128)(2,1)S(1)}, bf16[2048,128]{1,0:T(8,1...) custom-call(bf16[128,1024]{1,0:T(8,128)(2,1)} %in_ref.1, ...), custom_call_target="tpu_custom_call" | custom-call | tf_op jit(solution)/shard_map/ffn_backward/pallas_call | solution.py:566
  104.7 6.3 %widen.1 = (bf16[128,1024]{1,0:T(8,128)(2,1)}, f32[1024,2048]{1,0:T(8,128)}, f32[2048,1024]{1,0:T(8,128)}) custom-call(bf16[128,1024]{1,0:T(8,128)(2,1)S(1)} %get-tuple-element.20.gin_ref, bf16[2048,128]{1,0:T(8,128)(2,1)S(1)} %get-tuple-element.21.refs_0_, bf16[2048,128]{1,0:T(8,128)(2,1)S(1)} %get-tuple-element.22.refs_1_, ...), custom_call_target="tpu_custom_call" | custom-call | tf_op jit(solution)/shard_map/widen/pallas_call | solution.py:589

commit v7 on v6

--- a/solution.py
+++ b/solution.py
@@ -482,7 +482,7 @@
                 left = hops(RINGS[ring_of(lane, phase)], arm) - k
                 begin, rows = chunk(lane, phase, -left if arm == 0 else left)
                 add(g, 0, begin, (TABLE[lane, phase, arm, k][1],), rows)
-            if begun == len(LANES) and aside:
+            if begun == len(LANES) and aside and count % 3 == 0:
                 aside.pop(0)()
         else:
             phase = step[2]

time: 111 us -> 110 us (level)
  no operation moved by 1% of the time
where the time goes in v7:
time: 110 us
  Pallas kernels  109 us (99%)
    pallas_call x1, Pallas kernels, shards(): pl.pallas_call(body, name='ffn_backward', out_shape=(gin_shape, *(jax.Sha...  103 us
    pallas_call x1, Pallas kernels, shards(): pl.pallas_call(widen, name='widen', out_shape=(gin_shape, jax.ShapeDtypeS...  6.3 us

profile of v7, /device:TPU:8, one launch (start us, length us, event | category | flops | bytes accessed | tf_op | source)
XLA Modules:
  0.0 110.1 jit_solution(11373980252687654745)
XLA Ops:
  0.6 103.0 %ffn_backward.1 = (bf16[128,1024]{1,0:T(8,128)(2,1)S(1)}, bf16[2048,128]{1,0:T(8,128)(2,1)S(1)}, bf16[2048,128]{1,0:T(8,128)(2,1)S(1)}, bf16[2048,128]{1,0:T(8,1...) custom-call(bf16[128,1024]{1,0:T(8,128)(2,1)} %in_ref.1, ...), custom_call_target="tpu_custom_call" | custom-call | tf_op jit(solution)/shard_map/ffn_backward/pallas_call | solution.py:566
  103.6 6.3 %widen.1 = (bf16[128,1024]{1,0:T(8,128)(2,1)}, f32[1024,2048]{1,0:T(8,128)}, f32[2048,1024]{1,0:T(8,128)}) custom-call(bf16[128,1024]{1,0:T(8,128)(2,1)S(1)} %get-tuple-element.20.gin_ref, bf16[2048,128]{1,0:T(8,128)(2,1)S(1)} %get-tuple-element.21.refs_0_, bf16[2048,128]{1,0:T(8,128)(2,1)S(1)} %get-tuple-element.22.refs_1_, ...), custom_call_target="tpu_custom_call" | custom-call | tf_op jit(solution)/shard_map/widen/pallas_call | solution.py:589
